TPU v7x, 512 devices: a whole 4x8x8 slice. The times are simulated.
512 devices in a mesh: rep: 2 (over z_hi), fs: 32 (over z_lo, y), tp: 8 (over x, core).
Axes of the slice: x: 4, y: 8, z: 8 (z_hi: 2, z_lo: 4; z = z_hi * 4 + z_lo), core: 2. Of those that a mesh axis runs over, the one named last changes fastest.
Arguments:
- pre_gate: bfloat16 [49152, 4096], P(('rep', 'fs'), 'tp'), may hold values from -6 to 6
- pre_linear: bfloat16 [49152, 4096], P(('rep', 'fs'), 'tp'), may hold values from -6 to 6
- taps_gate: float32 [3, 4096], P(None, 'tp'), may hold values from -3.5 to 3.5
- taps_linear: float32 [3, 4096], P(None, 'tp'), may hold values from -3.5 to 3.5
- bias_gate: float32 [4096], P('tp'), may hold values from -3 to 3
- bias_linear: float32 [4096], P('tp'), may hold values from -3 to 3
- down_weight: bfloat16 [4096, 2048], P('tp', 'fs'), may hold values from -0.09375 to 0.09375
- out_grad: bfloat16 [49152, 2048], P(('rep', 'fs')), may hold values from -8 to 8
Outputs:
- grad_gate: bfloat16 [49152, 4096], P(('rep', 'fs'), 'tp')
- grad_linear: bfloat16 [49152, 4096], P(('rep', 'fs'), 'tp')
- grad_taps_gate: float32 [3, 4096], P(None, 'tp')
- grad_taps_linear: float32 [3, 4096], P(None, 'tp')
- grad_bias_gate: float32 [4096], P('tp')
- grad_bias_linear: float32 [4096], P('tp')
- grad_down: float32 [4096, 2048], P('tp', 'fs')
- row_norms: float32 [4096], P('tp')
All inputs are finite; a program needn't handle non-finite values.
Results may differ from a plain program's by a relative error of at most 0.0031.
Values may be sent and summed in bfloat16 or wider, within the bound.
A program may use at most 64 MiB of HBM per device.

v0:
```python
import jax
import jax.numpy as jnp
from jax import lax
from jax.sharding import Mesh
from jax.sharding import PartitionSpec as P

FS = ("fs_0", "fs_1")
REP_FS = ("rep", "fs_0", "fs_1")


def joined_along(parts, dim):
    lengths = list(parts.shape[1:])
    lengths[dim] *= parts.shape[0]
    return jnp.moveaxis(parts, 0, dim).reshape(lengths)


def copy_for_each(shard, axis):
    count = lax.axis_size(axis)
    return lax.all_to_all(
        jnp.broadcast_to(shard[None], (count, *shard.shape)), axis, 0, 0, tiled=True
    )


def gather_directly(shard, axis, dim):
    return joined_along(copy_for_each(shard, axis), dim)


def by_axis(shard, axes):
    for axis in axes:
        shard = lax.psum(shard, axis)
    return shard


def sum_in_order(parts, axes, sequence):
    inside = parts.shape[1:]
    parts = parts.reshape(*(lax.axis_size(a) for a in axes), *inside)
    parts = jnp.moveaxis(parts, sequence, range(len(axes))).reshape(-1, *inside)
    for k in sequence:
        parts = lax.psum_scatter(parts, axes[k], scatter_dimension=0, tiled=True)
    return parts[0]


def split_up(shard, dim, count):
    lengths = shard.shape
    parts = shard.reshape(*lengths[:dim], count, lengths[dim] // count, *lengths[dim + 1 :])
    return jnp.moveaxis(parts, dim, 0)


def scatter_axes(shard, axes, sequence, dim):
    count = lax.axis_size(axes)
    return sum_in_order(split_up(shard, dim, count), axes, sequence)


def of_everyone(shard, axis):
    everything = copy_for_each(shard, axis)
    return jnp.sum(everything, axis=0)


def convolve(values, taps, bias):
    length = values.shape[0]
    padded = jnp.pad(values, ((2, 0), (0, 0)))
    return (
        taps[0] * padded[0:length]
        + taps[1] * padded[1 : length + 1]
        + taps[2] * padded[2 : length + 2]
        + bias
    )


def convolve_back(grads, taps):
    length = grads.shape[0]
    padded = jnp.pad(grads, ((0, 2), (0, 0)))
    return (
        taps[0] * padded[2 : length + 2]
        + taps[1] * padded[1 : length + 1]
        + taps[2] * padded[0:length]
    )


def tap_grads(grads, values):
    length = values.shape[0]
    padded = jnp.pad(values, ((2, 0), (0, 0)))
    return jnp.stack([jnp.sum(grads * padded[j : j + length], axis=0) for j in range(3)])


def local(
    pre_gate, pre_linear, taps_gate, taps_linear, bias_gate, bias_linear, down_weight, out_grad
):
    gate_in = pre_gate.astype(jnp.float32)
    linear_in = pre_linear.astype(jnp.float32)
    gate_pre = convolve(gate_in, taps_gate, bias_gate)
    linear_pre = convolve(linear_in, taps_linear, bias_linear)
    sigma = jax.nn.sigmoid(gate_pre)
    silu_val = gate_pre * sigma
    hidden = (silu_val * linear_pre).astype(jnp.bfloat16)
    gathered = gather_directly(down_weight, FS, 1)
    grad_hidden = lax.dot_general(
        out_grad, gathered, (((1,), (1,)), ((), ())), preferred_element_type=jnp.float32
    )
    grad_gate_pre = grad_hidden * linear_pre * sigma * (1.0 + gate_pre * (1.0 - sigma))
    grad_linear_pre = grad_hidden * silu_val
    grad_gate = convolve_back(grad_gate_pre, taps_gate).astype(jnp.bfloat16)
    grad_linear = convolve_back(grad_linear_pre, taps_linear).astype(jnp.bfloat16)
    conv_parts = (
        tap_grads(grad_gate_pre, gate_in),
        tap_grads(grad_linear_pre, linear_in),
        jnp.sum(grad_gate_pre, axis=0),
        jnp.sum(grad_linear_pre, axis=0),
    )
    grad_taps_gate, grad_taps_linear, grad_bias_gate, grad_bias_linear = (
        by_axis(conv_parts[0], REP_FS),
        by_axis(conv_parts[1], REP_FS),
        by_axis(conv_parts[2], REP_FS),
        by_axis(conv_parts[3], REP_FS),
    )
    partial_grad = scatter_axes(
        lax.dot_general(
            out_grad, hidden, (((0,), (0,)), ((), ())), preferred_element_type=jnp.float32
        ),
        FS,
        (1, 0),
        0,
    )
    summed = of_everyone(partial_grad, "rep")
    grad_down = summed.T
    row_norms = by_axis(jnp.sum(grad_down * grad_down, axis=1), FS)
    return (
        grad_gate,
        grad_linear,
        grad_taps_gate,
        grad_taps_linear,
        grad_bias_gate,
        grad_bias_linear,
        grad_down,
        row_norms,
    )


def solution(mesh):
    split = Mesh(
        mesh.devices.reshape(mesh.shape["rep"], 4, 8, mesh.shape["tp"]),
        ("rep", "fs_0", "fs_1", "tp"),
    )
    in_specs = (
        P(REP_FS, "tp"),
        P(REP_FS, "tp"),
        P(None, "tp"),
        P(None, "tp"),
        P("tp"),
        P("tp"),
        P("tp", FS),
        P(REP_FS, None),
    )
    out_specs = (
        P(REP_FS, "tp"),
        P(REP_FS, "tp"),
        P(None, "tp"),
        P(None, "tp"),
        P("tp"),
        P("tp"),
        P("tp", FS),
        P("tp"),
    )
    return jax.shard_map(local, mesh=split, in_specs=in_specs, out_specs=out_specs, check_vma=False)
```

profile of v0, /device:TPU:6, one launch (start us, length us, event | category | flops | bytes accessed | tf_op | source)
XLA Modules:
  0.0 260.8 jit_solution(16937942078931800513)
XLA Ops:
  7.2 0.0 copy-start
  7.2 2.5 broadcast_in_dim.6
  9.7 13.0 %all-to-all-start = ((bf16[32,512,64]{1,2,0:T(8,128)(2,1)}), bf16[32,512,64]{1,2,0:T(8,128)(2,1)}, u32[]{:S(2)}, u32[]{:S(2)}) async-start(bf16[32,512,64]{1,2,0:T(8,128)(2,1)} %broadcast_in_dim.6), calls=%async_computation | async-start | bytes 4194304 | tf_op jit(solution)/shard_map/all_to_all | solution.py:19
  22.8 0.0 reduce-scatter.3.cloned.1.call-start
  22.8 0.0 copy-start.4
  22.8 2.6 convert_element_type.24
  25.4 0.0 copy-done.4
  25.4 1.4 convert_element_type.23
  26.8 0.0 copy-done.6
  26.9 0.0 copy-done.7
  26.9 46.6 %all-to-all-done = bf16[32,512,64]{1,2,0:T(8,128)(2,1)} async-done(((bf16[32,512,64]{1,2,0:T(8,128)(2,1)}), bf16[32,512,64]{1,2,0:T(8,128)(2,1)}, u32[]{:S(2)}, u32[]{:S(2)}) %all-to-all-start) | async-done | bytes 2097184 | tf_op jit(solution)/shard_map/all_to_all | solution.py:19
  73.5 0.0 copy-done
  73.5 0.0 copy-start.3
  73.5 0.0 copy-start.8
  73.5 7.1 %fusion.4 = (f32[512]{0:T(512)S(1)}, f32[512]{0:T(512)S(1)}, f32[512]{0:T(512)S(1)}, f32[512]{0:T(512)S(1)}, f32[768,512]{1,0:T(8,128)S(1)}, /*index=5*/f32[768,512]{1,0:T(8,128)S(1)}, f32[768,512]{1,0:T(8,128)S(1)}) fusion(bf16[768,512]{1,0:T(8,128)(2,1)} %param.9, f32[768,512]{1,0:T(8,128)} %convert_element_type.23, f32[512]{0:T(512)S(1)} %copy-done.9, ...), kind=kOutput, calls=%fused_computation.24 | convolution fusion | flops 1618081792 | bytes 13910016 | tf_op jit(solution)/shard_map/dot_general | solution.py:97
  80.7 3.2 %fusion.5 = (f32[512]{0:T(512)S(1)}, f32[512]{0:T(512)S(1)}, f32[512]{0:T(512)S(1)}, f32[512]{0:T(512)S(1)}, f32[768,512]{1,0:T(8,128)}, /*index=5*/f32[768,512]{1,0:T(8,128)S(1)}, bf16[768,512]{1,0:T(8,128)(2,1)}) fusion(bf16[768,512]{1,0:T(8,128)(2,1)S(1)} %copy-done.3, f32[768,512]{1,0:T(8,128)S(1)} %copy-done.1, f32[768,512]{1,0:T(8,128)S(1)} %get-tuple-element.35, ...), kind=kLoop, calls=%fused_computation.25 | loop fusion | flops 11401216 | bytes 12599296 | tf_op jit(solution)/shard_map/reduce_sum | solution.py:107
  83.9 3.9 %convolution_bitcast_fusion = f32[2048,512]{0,1:T(8,128)} fusion(bf16[768,2048]{1,0:T(8,128)(2,1)S(1)} %copy-done, f32[768,512]{1,0:T(8,128)S(1)} %get-tuple-element.37, f32[768,512]{1,0:T(8,128)S(1)} %get-tuple-element.35), kind=kOutput, calls=%fused_computation | convolution fusion | flops 1612972032 | bytes 10485760 | tf_op jit(solution)/shard_map/dot_general | solution.py:117
  87.9 5.3 %copy.19 = f32[2048,512]{1,0:T(8,128)} copy(f32[2048,512]{0,1:T(8,128)} %convolution_bitcast_fusion) | data formatting | bytes 8388608 | tf_op jit(solution)/shard_map/dot_general | solution.py:117
  93.2 4.9 %copy.20 = f32[8,4,64,512]{3,2,1,0:T(8,128)} copy(f32[8,4,64,512]{3,2,0,1:T(8,128)} %bitcast.28) | data formatting | bytes 8388608 | tf_op jit(solution)/shard_map/transpose | solution.py:37
  98.1 0.0 reduce-scatter.3.cloned.1.call-update
  98.1 0.0 reduce-scatter.5.cloned.1.call-start
  98.2 58.8 %reduce-scatter.3.cloned.1.call-done = f32[4,64,512]{2,1,0:T(8,128)} async-done(((f32[32,64,512]{2,1,0:T(8,128)}), f32[4,64,512]{2,1,0:T(8,128)}) %reduce-scatter.3.cloned.1.call-update) | async-done | bytes 524304 | tf_op jit(solution)/shard_map/reduce_scatter | solution.py:39
  156.9 0.0 reduce-scatter.5.cloned.1.call-update
  157.0 17.4 %all-reduce.6 = (f32[3,512]{1,0:T(4,128)S(1)}, f32[3,512]{1,0:T(4,128)S(1)}, f32[512]{0:T(512)}, f32[512]{0:T(512)}) all-reduce(f32[3,512]{1,0:T(4,128)S(1)} %get-tuple-element.46, f32[3,512]{1,0:T(4,128)S(1)} %get-tuple-element.47, f32[512]{0:T(512)S(1)} %get-tuple-element.16, ...), channel_id=1, replica_groups=mesh['rep'=2,'fs_0'=4,'fs_1'=8,'tp'=8] {'rep'}, use_global_device_ids=true, to_apply=%region_3.4 | all-reduce | flops 4096 | bytes 32768 | tf_op jit(solution)/shard_map/psum | solution.py:30
  174.4 14.6 %reduce-scatter.5.cloned.1.call-done = f32[1,64,512]{2,1,0:T(8,128)} async-done(((f32[4,64,512]{2,1,0:T(8,128)}), f32[1,64,512]{2,1,0:T(8,128)}) %reduce-scatter.5.cloned.1.call-update) | async-done | bytes 131088 | tf_op jit(solution)/shard_map/reduce_scatter | solution.py:39
  189.1 1.6 broadcast_in_dim.8
  190.7 4.1 %all-to-all-start.1 = ((f32[2,64,512]{2,1,0:T(8,128)}), f32[2,64,512]{2,1,0:T(8,128)S(1)}, u32[]{:S(2)}, u32[]{:S(2)}) async-start(f32[2,64,512]{2,1,0:T(8,128)} %broadcast_in_dim.8), calls=%async_computation.3 | async-start | bytes 524288 | tf_op jit(solution)/shard_map/all_to_all | solution.py:19
  194.8 4.1 %add_convert_fusion.1 = bf16[768,512]{1,0:T(8,128)(2,1)} fusion(f32[768,512]{1,0:T(8,128)} %get-tuple-element.36, f32[512]{0:T(512)S(1)} %bitcast.40, f32[512]{0:T(512)S(1)} %bitcast.42, f32[512]{0:T(512)S(1)} %bitcast.38), kind=kLoop, calls=%fused_computation.9 | loop fusion | flops 2359296 | bytes 2365440 | tf_op jit(solution)/shard_map/convert_element_type | solution.py:102
  198.9 5.6 %all-to-all-done.1 = f32[2,64,512]{2,1,0:T(8,128)S(1)} async-done(((f32[2,64,512]{2,1,0:T(8,128)}), f32[2,64,512]{2,1,0:T(8,128)S(1)}, u32[]{:S(2)}, u32[]{:S(2)}) %all-to-all-start.1) | async-done | bytes 262176 | tf_op jit(solution)/shard_map/all_to_all | solution.py:19
  204.5 0.0 copy-start.5
  204.5 19.2 %all-reduce.5 = (f32[3,512]{1,0:T(4,128)S(1)}, f32[3,512]{1,0:T(4,128)S(1)}, f32[512]{0:T(512)S(1)}, f32[512]{0:T(512)S(1)}, f32[512]{0:T(512)S(1)}) all-reduce(f32[3,512]{1,0:T(4,128)S(1)} %get-tuple-element.30, f32[3,512]{1,0:T(4,128)S(1)} %get-tuple-element.31, ...), channel_id=1, replica_groups=mesh['rep'=2,'fs_0'=4,'fs_1'=8,'tp'=8] {'fs_0'}, use_global_device_ids=true, to_apply=%region_4.5 | all-reduce | flops 4608 | bytes 36864 | tf_op jit(solution)/shard_map/psum | solution.py:30
  223.7 30.2 %all-reduce.4 = (f32[3,512]{1,0:T(4,128)}, f32[3,512]{1,0:T(4,128)}, f32[512]{0:T(512)}, f32[512]{0:T(512)}, f32[512]{0:T(512)}) all-reduce(f32[3,512]{1,0:T(4,128)S(1)} %get-tuple-element.25, f32[3,512]{1,0:T(4,128)S(1)} %get-tuple-element.26, ...), channel_id=1, replica_groups=mesh['rep'=2,'fs_0'=4,'fs_1'=8,'tp'=8] {'fs_1'}, use_global_device_ids=true, to_apply=%region_5.6 | all-reduce | flops 4608 | bytes 36864 | tf_op jit(solution)/shard_map/psum | solution.py:30
  (16 shorter events, 0.1 us)
Async XLA Ops:
  7.2 66.3 %copy-start = (bf16[768,2048]{1,0:T(8,128)(2,1)S(1)}, bf16[768,2048]{1,0:T(8,128)(2,1)}, u32[]{:S(2)}) copy-start(bf16[768,2048]{1,0:T(8,128)(2,1)} %param.15) | copy-start | bytes 9437188
  9.7 63.8 %all-to-all-start = ((bf16[32,512,64]{1,2,0:T(8,128)(2,1)}), bf16[32,512,64]{1,2,0:T(8,128)(2,1)}, u32[]{:S(2)}, u32[]{:S(2)}) async-start(bf16[32,512,64]{1,2,0:T(8,128)(2,1)} %broadcast_in_dim.6), calls=%async_computation | async-start | bytes 4194304 | tf_op jit(solution)/shard_map/all_to_all | solution.py:19
  22.8 134.2 %reduce-scatter.3.cloned.1.call-start = ((), (), s32[]{:S(2)}) async-start(), calls=%async_computation.4 | async-start | bytes 4718592 | tf_op jit(solution)/shard_map/reduce_scatter | solution.py:39
  22.8 2.6 %copy-start.4 = (bf16[768,512]{1,0:T(8,128)(2,1)S(1)}, bf16[768,512]{1,0:T(8,128)(2,1)}, u32[]{:S(2)}) copy-start(bf16[768,512]{1,0:T(8,128)(2,1)} %param.9) | copy-start | bytes 2359300
  25.4 1.4 copy-start.6
  25.4 1.4 copy-start.7
  25.4 48.1 %copy-start.9 = (f32[512]{0:T(512)S(1)}, f32[512]{0:T(512)}, u32[]{:S(2)}) copy-start(f32[512]{0:T(512)} %param.12) | copy-start | bytes 6148
  73.5 7.1 %copy-start.1 = (f32[768,512]{1,0:T(8,128)S(1)}, f32[768,512]{1,0:T(8,128)}, u32[]{:S(2)}) copy-start(f32[768,512]{1,0:T(8,128)} %convert_element_type.24) | copy-start | bytes 4718596
  73.5 7.1 %copy-start.2 = (f32[768,512]{1,0:T(8,128)S(1)}, f32[768,512]{1,0:T(8,128)}, u32[]{:S(2)}) copy-start(f32[768,512]{1,0:T(8,128)} %convert_element_type.23) | copy-start | bytes 4718596
  73.5 7.2 %copy-start.3 = (bf16[768,512]{1,0:T(8,128)(2,1)S(1)}, bf16[768,512]{1,0:T(8,128)(2,1)}, u32[]{:S(2)}) copy-start(bf16[768,512]{1,0:T(8,128)(2,1)} %param.8) | copy-start | bytes 2359300
  73.5 7.1 %copy-start.8 = (f32[512]{0:T(512)S(1)}, f32[512]{0:T(512)}, u32[]{:S(2)}) copy-start(f32[512]{0:T(512)} %param.13) | copy-start | bytes 6148
  98.1 90.9 %reduce-scatter.5.cloned.1.call-start = ((), (), s32[]{:S(2)}) async-start(), calls=%async_computation.5 | async-start | bytes 655360 | tf_op jit(solution)/shard_map/reduce_scatter | solution.py:39
  190.7 13.8 %all-to-all-start.1 = ((f32[2,64,512]{2,1,0:T(8,128)}), f32[2,64,512]{2,1,0:T(8,128)S(1)}, u32[]{:S(2)}, u32[]{:S(2)}) async-start(f32[2,64,512]{2,1,0:T(8,128)} %broadcast_in_dim.8), calls=%async_computation.3 | async-start | bytes 524288 | tf_op jit(solution)/shard_map/all_to_all | solution.py:19
  204.5 49.5 %copy-start.5 = (f32[64,512]{1,0:T(8,128)}, f32[64,512]{1,0:T(8,128)S(1)}, u32[]{:S(2)}) copy-start(f32[64,512]{1,0:T(8,128)S(1)} %reduce_sum.98) | copy-start | bytes 393220
Sparse Core Ops, SparseCore 0:
  98.2 58.6 reduce-scatter.2
  159.7 29.2 reduce-scatter.4
where the time goes:
time: 261 us
  waiting for transfers between devices  126 us (48%)
  blocking collectives  66.9 us (26%)
  starting transfers between devices  17.2 us (7%)
  local copies, waits for them, and re-layouts  14.4 us (6%)
  between operations  14.2 us (5%)
  other arithmetic  11.4 us (4%)
  matrix products  11 us (4%)
    reduce_scatter x2, waiting for transfers between devices, sum_in_order(): parts = lax.psum_scatter(parts, axes[k], scatter_dimension=0, tiled=True)  73.4 us
    psum x3, blocking collectives, by_axis(): shard = lax.psum(shard, axis)  66.9 us
    all_to_all x2, waiting for transfers between devices, copy_for_each(): lax.all_to_all(jnp.broadcast_to(shard[None], (count, *shard.shape)), axis...  52.2 us
    all_to_all x2, starting transfers between devices, copy_for_each(): lax.all_to_all(jnp.broadcast_to(shard[None], (count, *shard.shape)), axis...  17.1 us
    dot_general x1, matrix products, local(): lax.dot_general(out_grad, gathered, (((1,), (1,)), ((), ())), preferred_e...  7.1 us
    dot_general x1, local copies, waits for them, and re-layouts, local(): lax.dot_general(out_grad, hidden, (((0,), (0,)), ((), ())), preferred_ele...  5.35 us
  transfers between devices with their start and end apart: 4, of which 4 were waited for; matrix products, arithmetic and copies ran while one was open for 3% of the time, Pallas kernels for 0%

commit v1 on v0

v1 whole, which is shorter than its diff:
```python
import jax
import jax.numpy as jnp
from jax import lax
from jax.experimental import pallas as pl
from jax.experimental.pallas import tpu as pltpu
from jax.sharding import Mesh
from jax.sharding import PartitionSpec as P

REP_FS = ("rep", "fs_0", "fs_1")
RING = 8
BLOCK = 64
HALF = 256
ROWS = 32
F32, BF16 = jnp.float32, jnp.bfloat16
FAR_FIRST = (4, 3, 5, 2, 6, 1, 7)


def gather_messages():
    found = []

    def add(half, dz, dy, part, axis, sign, needs):
        found.append((half, dz, dy, part, axis, sign, needs))
        return len(found) - 1

    right = add(0, 0, 0, 0, "z", 1, ())
    left = add(0, 0, 0, 0, "z", -1, ())
    right2 = add(0, -1, 0, 1, "z", 1, (right,))
    left2 = add(0, 1, 0, 2, "z", -1, (left,))
    for j, (dz, needs) in enumerate(
        ((0, ()), (-1, (right,)), (1, (left,)), (2, (right2, left2)))
    ):
        for sign, hops in ((1, 4 - j % 2), (-1, 3 + j % 2)):
            before = needs
            for k in range(hops):
                before = (add(0, dz, -sign * k, 0, "y", sign, before),)
    items = [(0, ())]
    for sign, hops in ((1, 4), (-1, 3)):
        before = ()
        for k in range(hops):
            before = (add(1, 0, -sign * k, 0, "y", sign, before),)
            items.append((-sign * (k + 1), before))
    for i, (dy, needs) in enumerate(items):
        first = add(1, 0, dy, 0, "z", 1, needs)
        other = add(1, 0, dy, 0, "z", -1, needs)
        if i % 2 == 0:
            add(1, -1, dy, 0, "z", 1, (first,))
        else:
            add(1, 1, dy, 0, "z", -1, (other,))
    return found


GATHER = gather_messages()
ROUND = []
for _m in GATHER:
    ROUND.append(1 + max((ROUND[k] for k in _m[6]), default=-1))
LAST_ROUND = max(ROUND)


def chain_messages():
    return [
        (half, part, sign, step, hops)
        for half in range(2)
        for part in range(2)
        for sign, hops in ((1, 4 - part), (-1, 3 + part))
        for step in range(hops)
    ]


CHAIN = chain_messages()
CHAIN_AT = {m[:4]: k for k, m in enumerate(CHAIN)}


def kernel(
    gate_hbm, linear_hbm, taps_g, taps_l, bias_g, bias_l, weight_hbm, out_grad_hbm,
    gg_hbm, gl_hbm, taps_g_out, taps_l_out, bias_g_out, bias_l_out, down_out, norms_out,
    gate, linear, out_grad, weights, hidden, factor_g, factor_l, grad_hidden, partial,
    gg, gl, chain_send, chain_recv, summed, cross_send, cross_recv, final, other_final,
    conv_send, conv_y, conv_z, norm_send, norm_y, norm_z,
    load_sem, store_sem, gather_s, gather_r, chain_s, chain_r, cross_s, cross_r,
    small_s, small_r, swap_s, swap_r,
):
    tokens = gate_hbm.shape[0]
    rep, z_lo, y = lax.axis_index("rep"), lax.axis_index("fs_0"), lax.axis_index("fs_1")
    z = rep * 4 + z_lo

    def along(axis, shift):
        if axis == "y":
            return {"fs_1": lax.rem(y + shift + RING, RING)}
        at = lax.rem(z + shift + RING, RING)
        return {"rep": at // 4, "fs_0": lax.rem(at, 4)}

    def remote(src, dst, send, recv, axis, shift):
        return pltpu.make_async_remote_copy(
            src_ref=src, dst_ref=dst, send_sem=send, recv_sem=recv,
            device_id=along(axis, shift), device_id_type=pl.DeviceIdType.MESH,
        )

    barrier = pltpu.get_barrier_semaphore()
    for axis in ("y", "z"):
        for shift in range(1, RING):
            pl.semaphore_signal(
                barrier, inc=1, device_id=along(axis, shift),
                device_id_type=pl.DeviceIdType.MESH,
            )

    own_row = pl.multiple_of((z_lo * 8 + y) * BLOCK, BLOCK)
    loads = [
        pltpu.make_async_copy(
            weight_hbm.at[:, pl.ds(h * HALF, HALF)],
            weights.at[h, pl.ds(own_row, BLOCK), :],
            load_sem.at[h],
        )
        for h in range(2)
    ]
    loads += [
        pltpu.make_async_copy(gate_hbm, gate.at[pl.ds(16, tokens), :], load_sem.at[2]),
        pltpu.make_async_copy(linear_hbm, linear.at[pl.ds(16, tokens), :], load_sem.at[3]),
        pltpu.make_async_copy(out_grad_hbm, out_grad, load_sem.at[4]),
    ]
    for load in loads:
        load.start()
    for ref in (gate, linear):
        ref[0:16, :] = jnp.zeros((16, ref.shape[1]), BF16)

    def gather_copy(k):
        half, dz, dy, part, axis, sign, _ = GATHER[k]
        at = lax.rem(z_lo + dz + 4, 4) * 8 + lax.rem(y + dy + RING, RING)
        start, size = at * BLOCK, BLOCK
        if part:
            start, size = start + (part - 1) * 32, 32
        block = weights.at[half, pl.ds(pl.multiple_of(start, size), size), :]
        return remote(block, block, gather_s.at[k], gather_r.at[k], axis, sign)

    def gather_round(number):
        arrived = set(k for k, r in enumerate(ROUND) if r < number - 1)
        todo = [k for k, r in enumerate(ROUND) if r == number]
        for k in [k for k, r in enumerate(ROUND) if r == number - 1]:
            gather_copy(k).wait_recv()
            arrived.add(k)
            for m in list(todo):
                if all(n in arrived for n in GATHER[m][6]):
                    gather_copy(m).start()
                    todo.remove(m)
        for m in todo:
            gather_copy(m).start()

    STEP = 32

    def shifted(ref, row, lanes):
        rows = ref[pl.ds(row, STEP + 16), lanes].astype(F32)
        return pltpu.roll(rows, 2, 0)[16:], pltpu.roll(rows, 1, 0)[16:], rows[16:]

    def forward(half):
        lanes = slice(half * HALF, (half + 1) * HALF)
        tg, tl = taps_g[0:3, lanes], taps_l[0:3, lanes]
        bg, bl = bias_g[0:1, lanes], bias_l[0:1, lanes]

        def body(i, carry):
            row = pl.multiple_of(i * STEP, STEP)
            g0, g1, g2 = shifted(gate, row, lanes)
            l0, l1, l2 = shifted(linear, row, lanes)
            gate_pre = tg[0:1] * g0 + tg[1:2] * g1 + tg[2:3] * g2 + bg
            linear_pre = tl[0:1] * l0 + tl[1:2] * l1 + tl[2:3] * l2 + bl
            sigma = 1.0 / (1.0 + jnp.exp(-gate_pre))
            silu = gate_pre * sigma
            hidden[pl.ds(row, STEP), lanes] = (silu * linear_pre).astype(BF16)
            factor_g[pl.ds(row, STEP), lanes] = (
                linear_pre * sigma * (1.0 + gate_pre * (1.0 - sigma))
            )
            factor_l[pl.ds(row, STEP), lanes] = silu
            return carry

        lax.fori_loop(0, tokens // STEP, body, 0)

    def weight_grad(half):
        lanes = slice(half * HALF, (half + 1) * HALF)

        def body(i, carry):
            at = pl.multiple_of(i * 512, 512)
            partial[half, pl.ds(at, 512), :] = lax.dot_general(
                out_grad[:, pl.ds(at, 512)], hidden[:, lanes],
                (((0,), (0,)), ((), ())), preferred_element_type=F32,
            )
            return carry

        lax.fori_loop(0, 4, body, 0)

    def hidden_grad(half):
        lanes = slice(half * HALF, (half + 1) * HALF)

        def body(i, carry):
            at = pl.multiple_of(i * 256, 256)
            grad_hidden[pl.ds(at, 256), lanes] = jnp.dot(
                out_grad[pl.ds(at, 256), :], weights[half], preferred_element_type=F32
            )
            return carry

        lax.fori_loop(0, tokens // 256, body, 0)

    def fold(v):
        return jnp.sum(v.reshape(STEP // 8, 8, HALF), axis=0)

    def backward(half):
        lanes = slice(half * HALF, (half + 1) * HALF)
        tg, tl = taps_g[0:3, lanes], taps_l[0:3, lanes]

        def back(v, after, taps):
            longer = jnp.concatenate([v, after], axis=0)
            one = pltpu.roll(longer, STEP + 7, 0)[0:STEP]
            two = pltpu.roll(longer, STEP + 6, 0)[0:STEP]
            return taps[0:1] * two + taps[1:2] * one + taps[2:3] * v

        def body(i, carry):
            after_g, after_l, sums = carry
            row = pl.multiple_of((tokens // STEP - 1 - i) * STEP, STEP)
            grad = grad_hidden[pl.ds(row, STEP), lanes]
            dg = grad * factor_g[pl.ds(row, STEP), lanes]
            dl = grad * factor_l[pl.ds(row, STEP), lanes]
            gs = shifted(gate, row, lanes)
            ls = shifted(linear, row, lanes)
            gg[pl.ds(row, STEP), lanes] = back(dg, after_g, tg).astype(BF16)
            gl[pl.ds(row, STEP), lanes] = back(dl, after_l, tl).astype(BF16)
            terms = [dg * v for v in gs] + [dl * v for v in ls] + [dg, dl]
            sums = tuple(s + fold(t) for s, t in zip(sums, terms))
            return dg[0:8], dl[0:8], sums

        zero = jnp.zeros((8, HALF), F32)
        _, _, sums = lax.fori_loop(0, tokens // STEP, body, (zero, zero, (zero,) * 8))
        for j, s in enumerate(sums):
            conv_send[j : j + 1, lanes] = jnp.sum(s, axis=0, keepdims=True)

    def first_axis(half):
        return ("y", y) if half == 0 else ("z", z)

    def pieces(half, to, part):
        if half == 0:
            return [((2 * part + q) * 512 + to * 64, 64) for q in range(2)]
        return [
            (lax.rem(to, 4) * 512 + (4 * part + q) * 64 + (to // 4) * 32, 32)
            for q in range(4)
        ]

    def chain_copy(k):
        half, part, sign, step, hops = CHAIN[k]
        return remote(
            chain_send.at[k], chain_recv.at[k], chain_s.at[k], chain_r.at[k],
            first_axis(half)[0], sign,
        )

    def chain_step(half, step):
        for part in range(2):
            for sign, hops in ((1, 4 - part), (-1, 3 + part)):
                if step >= hops:
                    continue
                k = CHAIN_AT[half, part, sign, step]
                to = lax.rem(first_axis(half)[1] + sign * (hops - step) + RING, RING)
                if step:
                    chain_copy(k - 1).wait_recv()
                at = 0
                for row, size in pieces(half, to, part):
                    value = partial[half, pl.ds(pl.multiple_of(row, size), size), :]
                    if step:
                        value = value + chain_recv[k - 1, at : at + size, :].astype(F32)
                    chain_send[k, at : at + size, :] = value.astype(BF16)
                    at += size
                chain_copy(k).start()

    def chain_end(half):
        for part in range(2):
            ends = [
                CHAIN_AT[half, part, sign, hops - 1]
                for sign, hops in ((1, 4 - part), (-1, 3 + part))
            ]
            for k in ends:
                chain_copy(k).wait_recv()
            at = 0
            for row, size in pieces(half, first_axis(half)[1], part):
                value = partial[half, pl.ds(pl.multiple_of(row, size), size), :]
                for k in ends:
                    value = value + chain_recv[k, at : at + size, :].astype(F32)
                for sub in range(size // ROWS):
                    slot = (part * 128 + at) // ROWS + sub
                    piece = value[sub * ROWS : (sub + 1) * ROWS]
                    summed[half, slot] = piece
                    cross_send[half, slot] = piece.astype(BF16)
                at += size

    def slot_of(half, at):
        return lax.rem(at, 4) * 2 + at // 4 if half == 0 else at

    def cross_copy(half, shift):
        axis, here = ("z", z) if half == 0 else ("y", y)
        slot = slot_of(half, lax.rem(here + shift, RING))
        return remote(
            cross_send.at[half, slot], cross_recv.at[half, shift],
            cross_s.at[half, shift], cross_r.at[half, shift], axis, shift,
        )

    def cross_start(half):
        for shift in FAR_FIRST:
            cross_copy(half, shift).start()

    def cross_end(half):
        here = z if half == 0 else y
        value = summed[half, slot_of(half, here)]
        for shift in FAR_FIRST:
            cross_copy(half, shift).wait_recv()
        for shift in FAR_FIRST:
            value = value + cross_recv[half, shift].astype(F32)
        final[:, half * HALF : (half + 1) * HALF] = value

    def swap_copy():
        return remote(final, other_final, swap_s.at[0], swap_r.at[0], "z", 4)

    def small_copies(kind, axis, src, dst):
        here = y if axis == "y" else z
        base = (kind * 2 + (axis == "z")) * RING
        size = 8 if kind == 0 else 1
        return [
            remote(
                src.at[pl.ds(0, size), :], dst.at[here, pl.ds(0, size), :],
                small_s.at[base + shift], small_r.at[base + shift], axis, shift,
            )
            for shift in FAR_FIRST
        ]

    def small_start(kind, axis, src, dst):
        here = y if axis == "y" else z
        size = 8 if kind == 0 else 1
        for copy in small_copies(kind, axis, src, dst):
            copy.start()
        dst[here, 0:size, :] = src[0:size, :]

    def small_end(kind, axis, src, dst):
        size = 8 if kind == 0 else 1
        for copy in small_copies(kind, axis, src, dst):
            copy.wait_recv()
        value = dst[0, 0:size, :]
        for k in range(1, RING):
            value = value + dst[k, 0:size, :]
        return value

    loads[0].wait()
    loads[1].wait()
    pl.semaphore_wait(barrier, 2 * (RING - 1))
    gather_round(0)
    loads[2].wait()
    loads[3].wait()
    forward(0)
    gather_round(1)
    loads[4].wait()
    weight_grad(0)
    chain_step(0, 0)
    gather_round(2)
    forward(1)
    weight_grad(1)
    chain_step(1, 0)
    gather_round(3)
    chain_step(0, 1)
    chain_step(1, 1)
    gather_round(4)
    chain_step(0, 2)
    chain_step(1, 2)
    gather_round(5)
    chain_step(0, 3)
    chain_step(1, 3)
    for number in range(6, LAST_ROUND + 2):
        gather_round(number)
    hidden_grad(0)
    chain_end(0)
    cross_start(0)
    chain_end(1)
    cross_start(1)
    hidden_grad(1)
    backward(0)
    backward(1)
    small_start(0, "y", conv_send, conv_y)
    stores = [
        pltpu.make_async_copy(gg, gg_hbm, store_sem.at[0]),
        pltpu.make_async_copy(gl, gl_hbm, store_sem.at[1]),
    ]
    for store in stores:
        store.start()
    cross_end(0)
    cross_end(1)
    swap_copy().start()
    norm_send[0:1, :] = jnp.sum(final[...] * final[...], axis=0, keepdims=True)
    small_start(1, "y", norm_send, norm_y)
    conv = small_end(0, "y", conv_send, conv_y)
    conv_send2 = conv_z.at[RING]
    conv_send2[...] = conv
    small_start(0, "z", conv_send2, conv_z)
    norm = small_end(1, "y", norm_send, norm_y)
    norm_send2 = norm_z.at[RING]
    norm_send2[0:1, :] = norm
    small_start(1, "z", norm_send2, norm_z)
    conv = small_end(0, "z", conv_send2, conv_z)
    taps_g_out[...] = conv[0:3]
    taps_l_out[...] = conv[3:6]
    bias_g_out[...] = conv[6:7]
    bias_l_out[...] = conv[7:8]
    swap_copy().wait_recv()
    down_out[pl.ds(pl.multiple_of(rep * ROWS, ROWS), ROWS), :] = final[...]
    down_out[pl.ds(pl.multiple_of((1 - rep) * ROWS, ROWS), ROWS), :] = other_final[...]
    norms_out[...] = small_end(1, "z", norm_send2, norm_z)

    for k in range(len(GATHER)):
        gather_copy(k).wait_send()
    for k in range(len(CHAIN)):
        chain_copy(k).wait_send()
    for half in range(2):
        for shift in FAR_FIRST:
            cross_copy(half, shift).wait_send()
    swap_copy().wait_send()
    for kind, axis, src, dst in (
        (0, "y", conv_send, conv_y), (0, "z", conv_send2, conv_z),
        (1, "y", norm_send, norm_y), (1, "z", norm_send2, norm_z),
    ):
        for copy in small_copies(kind, axis, src, dst):
            copy.wait_send()
    for store in stores:
        store.wait()


def local(
    pre_gate, pre_linear, taps_gate, taps_linear, bias_gate, bias_linear, down_weight, out_grad
):
    tokens, width = pre_gate.shape
    columns = out_grad.shape[1]
    any_, vmem = pl.BlockSpec(memory_space=pl.ANY), pl.BlockSpec(memory_space=pltpu.VMEM)
    dma = pltpu.SemaphoreType.DMA
    shape = jax.ShapeDtypeStruct
    out = pl.pallas_call(
        kernel,
        name="gated_backward",
        out_shape=(
            shape((tokens, width), BF16), shape((tokens, width), BF16),
            shape((3, width), F32), shape((3, width), F32),
            shape((1, width), F32), shape((1, width), F32),
            shape((BLOCK, width), F32), shape((1, width), F32),
        ),
        in_specs=[any_, any_, vmem, vmem, vmem, vmem, any_, any_],
        out_specs=(any_, any_, vmem, vmem, vmem, vmem, vmem, vmem),
        scratch_shapes=[
            pltpu.VMEM((tokens + 16, width), BF16),
            pltpu.VMEM((tokens + 16, width), BF16),
            pltpu.VMEM((tokens, columns), BF16),
            pltpu.VMEM((2, columns, HALF), BF16),
            pltpu.VMEM((tokens, width), BF16),
            pltpu.VMEM((tokens, width), F32),
            pltpu.VMEM((tokens, width), F32),
            pltpu.VMEM((tokens, width), F32),
            pltpu.VMEM((2, columns, HALF), F32),
            pltpu.VMEM((tokens, width), BF16),
            pltpu.VMEM((tokens, width), BF16),
            pltpu.VMEM((len(CHAIN), 128, HALF), BF16),
            pltpu.VMEM((len(CHAIN), 128, HALF), BF16),
            pltpu.VMEM((2, RING, ROWS, HALF), F32),
            pltpu.VMEM((2, RING, ROWS, HALF), BF16),
            pltpu.VMEM((2, RING, ROWS, HALF), BF16),
            pltpu.VMEM((ROWS, width), F32),
            pltpu.VMEM((ROWS, width), F32),
            pltpu.VMEM((8, width), F32),
            pltpu.VMEM((RING, 8, width), F32),
            pltpu.VMEM((RING + 1, 8, width), F32),
            pltpu.VMEM((8, width), F32),
            pltpu.VMEM((RING, 8, width), F32),
            pltpu.VMEM((RING + 1, 8, width), F32),
            dma((5,)), dma((2,)),
            dma((len(GATHER),)), dma((len(GATHER),)),
            dma((len(CHAIN),)), dma((len(CHAIN),)),
            dma((2, RING)), dma((2, RING)),
            dma((4 * RING,)), dma((4 * RING,)),
            dma((1,)), dma((1,)),
        ],
        compiler_params=pltpu.CompilerParams(
            collective_id=0, has_side_effects=True, vmem_limit_bytes=60 * 2**20
        ),
    )(
        pre_gate, pre_linear, taps_gate, taps_linear,
        bias_gate.reshape(1, -1), bias_linear.reshape(1, -1), down_weight.T, out_grad,
    )
    gg, gl, tg, tl, bg, bl, down, norms = out
    return gg, gl, tg, tl, bg.reshape(-1), bl.reshape(-1), down.T, norms.reshape(-1)


def solution(mesh):
    split = Mesh(
        mesh.devices.reshape(mesh.shape["rep"], 4, 8, mesh.shape["tp"]),
        ("rep", "fs_0", "fs_1", "tp"),
    )
    fs = ("fs_0", "fs_1")
    in_specs = (
        P(REP_FS, "tp"), P(REP_FS, "tp"), P(None, "tp"), P(None, "tp"),
        P("tp"), P("tp"), P("tp", fs), P(REP_FS, None),
    )
    out_specs = (
        P(REP_FS, "tp"), P(REP_FS, "tp"), P(None, "tp"), P(None, "tp"),
        P("tp"), P("tp"), P("tp", fs), P("tp"),
    )
    return jax.shard_map(local, mesh=split, in_specs=in_specs, out_specs=out_specs, check_vma=False)
```

time: 261 us -> 71.9 us (0.28)
  waiting for transfers between devices: 126 us -> 0 us
  blocking collectives: 66.9 us -> 0 us
  Pallas kernels: 0 us -> 63 us
  starting transfers between devices: 17.2 us -> 0 us
  between operations: 14.2 us -> 0.7 us
  other arithmetic: 11.4 us -> 0 us
  matrix products: 11 us -> 0 us
  local copies, waits for them, and re-layouts: 14.4 us -> 7.77 us
    reduce_scatter x2 -> x0, waiting for transfers between devices: 73.4 us -> none  [sum_in_order(): parts = lax.psum_scatter(parts, axes[k], scatter_dimension=0, tiled=True)]
    psum x3 -> x0, blocking collectives: 66.9 us -> none  [by_axis(): shard = lax.psum(shard, axis)]
    pallas_call x0 -> x1, Pallas kernels: none -> 63 us  [local(): pl.pallas_call(kernel, name='gated_backward', out_shape=(shape((tokens, w...]
    all_to_all x2 -> x0, waiting for transfers between devices: 52.2 us -> none  [copy_for_each(): lax.all_to_all(jnp.broadcast_to(shard[None], (count, *shard.shape)), axis...]
    all_to_all x2 -> x0, starting transfers between devices: 17.1 us -> none  [copy_for_each(): lax.all_to_all(jnp.broadcast_to(shard[None], (count, *shard.shape)), axis...]
    dot_general x2 -> x0, matrix products: 11 us -> none  [the longest x1 7.1 us: local(): lax.dot_general(out_grad, gathered, (((1,), (1,)), ((), ())), preferred_e...]
    convert_element_type x3 -> x0, other arithmetic: 8.12 us -> none  [the longest x1 4.11 us: local(): grad_gate = convolve_back(grad_gate_pre, taps_gate).astype(jnp.bfloat16)]
    unnamed x20, local copies, waits for them, and re-layouts: 0.05 us -> 7.77 us
  transfers between devices with their start and end apart: 4 -> 0, of which waited for: 4 -> 0; matrix products, arithmetic and copies ran while one was open for 3% -> 0% of each run, Pallas kernels for 0% -> 0%
where the time goes in v1:
time: 71.9 us; the launch traced here: 71.5 us
  Pallas kernels  63 us (88%)
  local copies, waits for them, and re-layouts  7.77 us (11%)
    pallas_call x1, Pallas kernels, local(): pl.pallas_call(kernel, name='gated_backward', out_shape=(shape((tokens, w...  63 us
    unnamed x20, local copies, waits for them, and re-layouts  7.77 us

profile of v1, /device:TPU:6, one launch (start us, length us, event | category | flops | bytes accessed | tf_op | source)
XLA Modules:
  0.0 71.5 jit_solution(11247530649287658317)
XLA Ops:
  0.6 63.0 %gated_backward.1 = (bf16[768,512]{1,0:T(8,128)(2,1)}, bf16[768,512]{1,0:T(8,128)(2,1)}, f32[3,512]{1,0:T(4,128)}, f32[3,512]{1,0:T(4,128)}, f32[1,512]{1,0:T(1,...) custom-call(bf16[768,512]{1,0:T(8,128)(2,1)} %gate_hbm.1, bf16[768,512]{1,0:T(8,128)(2,1)} %linear_hbm.1, ...), custom_call_target="tpu_custom_call" | custom-call | tf_op jit(solution)/shard_map/gated_backward/pallas_call | solution.py:433
  63.6 0.0 copy-start.2
  63.7 0.0 copy-start.1
  63.7 0.0 copy-start.5
  63.7 0.0 copy-start.4
  63.7 0.0 copy-start
  63.7 0.0 copy-start.3
  63.7 2.1 %copy.24 = bf16[768,512]{1,0:T(8,128)(2,1)} copy(bf16[768,512]{1,0:T(8,128)(2,1)} %get-tuple-element.32) | data formatting | bytes 1572864
  65.8 2.1 %copy.25 = bf16[768,512]{1,0:T(8,128)(2,1)} copy(bf16[768,512]{1,0:T(8,128)(2,1)} %get-tuple-element.33) | data formatting | bytes 1572864
  67.9 0.0 copy-done.2
  67.9 0.6 copy.26
  68.5 0.0 copy-done.1
  68.5 0.6 copy.27
  69.1 0.0 copy-done.5
  69.1 0.6 copy.28
  69.7 0.0 copy-done.4
  69.7 0.6 copy.29
  70.2 0.0 copy-done
  70.2 0.7 copy.30
  70.9 0.0 copy-done.3
  70.9 0.6 copy.31
Async XLA Ops:
  63.6 4.2 %copy-start.2 = (f32[3,512]{1,0:T(4,128)S(1)}, f32[3,512]{1,0:T(4,128)}, u32[]{:S(2)}) copy-start(f32[3,512]{1,0:T(4,128)} %get-tuple-element.34) | copy-start | bytes 18436
  63.7 4.8 %copy-start.1 = (f32[3,512]{1,0:T(4,128)S(1)}, f32[3,512]{1,0:T(4,128)}, u32[]{:S(2)}) copy-start(f32[3,512]{1,0:T(4,128)} %get-tuple-element.35) | copy-start | bytes 18436
  63.7 5.4 %copy-start.5 = (f32[1,512]{1,0:T(1,128)S(1)}, f32[1,512]{1,0:T(1,128)}, u32[]{:S(2)}) copy-start(f32[1,512]{1,0:T(1,128)} %get-tuple-element.20) | copy-start | bytes 6148
  63.7 6.0 %copy-start.4 = (f32[1,512]{1,0:T(1,128)S(1)}, f32[1,512]{1,0:T(1,128)}, u32[]{:S(2)}) copy-start(f32[1,512]{1,0:T(1,128)} %get-tuple-element.21) | copy-start | bytes 6148
  63.7 6.5 %copy-start = (f32[64,512]{1,0:T(8,128)S(1)}, f32[64,512]{1,0:T(8,128)}, u32[]{:S(2)}) copy-start(f32[64,512]{1,0:T(8,128)} %get-tuple-element.22) | copy-start | bytes 393220
  63.7 7.2 %copy-start.3 = (f32[1,512]{1,0:T(1,128)S(1)}, f32[1,512]{1,0:T(1,128)}, u32[]{:S(2)}) copy-start(f32[1,512]{1,0:T(1,128)} %get-tuple-element.23) | copy-start | bytes 6148

commit v2 on v1

--- a/solution.py
+++ b/solution.py
@@ -71,12 +71,13 @@
 
 
 def kernel(
-    gate_hbm, linear_hbm, taps_g, taps_l, bias_g, bias_l, weight_hbm, out_grad_hbm,
-    gg_hbm, gl_hbm, taps_g_out, taps_l_out, bias_g_out, bias_l_out, down_out, norms_out,
-    gate, linear, out_grad, weights, hidden, factor_g, factor_l, grad_hidden, partial,
-    gg, gl, chain_send, chain_recv, summed, cross_send, cross_recv, final, other_final,
+    gate_hbm, linear_hbm, taps_g_hbm, taps_l_hbm, bias_g_hbm, bias_l_hbm, weight_hbm,
+    out_grad_hbm,
+    gg, gl, conv_out, down_out, norms_out,
+    gate, linear, taps_g, taps_l, bias_g, bias_l, out_grad, weights, hidden, factor_g, factor_l, grad_hidden, partial,
+    chain_send, chain_recv, summed, cross_send, cross_recv, final, other_final,
     conv_send, conv_y, conv_z, norm_send, norm_y, norm_z,
-    load_sem, store_sem, gather_s, gather_r, chain_s, chain_r, cross_s, cross_r,
+    load_sem, gather_s, gather_r, chain_s, chain_r, cross_s, cross_r,
     small_s, small_r, swap_s, swap_r,
 ):
     tokens = gate_hbm.shape[0]
@@ -115,6 +116,10 @@
     loads += [
         pltpu.make_async_copy(gate_hbm, gate.at[pl.ds(16, tokens), :], load_sem.at[2]),
         pltpu.make_async_copy(linear_hbm, linear.at[pl.ds(16, tokens), :], load_sem.at[3]),
+        pltpu.make_async_copy(taps_g_hbm, taps_g, load_sem.at[5]),
+        pltpu.make_async_copy(taps_l_hbm, taps_l, load_sem.at[6]),
+        pltpu.make_async_copy(bias_g_hbm, bias_g, load_sem.at[7]),
+        pltpu.make_async_copy(bias_l_hbm, bias_l, load_sem.at[8]),
         pltpu.make_async_copy(out_grad_hbm, out_grad, load_sem.at[4]),
     ]
     for load in loads:
@@ -344,11 +349,11 @@
     loads[1].wait()
     pl.semaphore_wait(barrier, 2 * (RING - 1))
     gather_round(0)
-    loads[2].wait()
-    loads[3].wait()
+    for load in loads[2:8]:
+        load.wait()
     forward(0)
     gather_round(1)
-    loads[4].wait()
+    loads[8].wait()
     weight_grad(0)
     chain_step(0, 0)
     gather_round(2)
@@ -375,12 +380,6 @@
     backward(0)
     backward(1)
     small_start(0, "y", conv_send, conv_y)
-    stores = [
-        pltpu.make_async_copy(gg, gg_hbm, store_sem.at[0]),
-        pltpu.make_async_copy(gl, gl_hbm, store_sem.at[1]),
-    ]
-    for store in stores:
-        store.start()
     cross_end(0)
     cross_end(1)
     swap_copy().start()
@@ -394,11 +393,7 @@
     norm_send2 = norm_z.at[RING]
     norm_send2[0:1, :] = norm
     small_start(1, "z", norm_send2, norm_z)
-    conv = small_end(0, "z", conv_send2, conv_z)
-    taps_g_out[...] = conv[0:3]
-    taps_l_out[...] = conv[3:6]
-    bias_g_out[...] = conv[6:7]
-    bias_l_out[...] = conv[7:8]
+    conv_out[...] = small_end(0, "z", conv_send2, conv_z)
     swap_copy().wait_recv()
     down_out[pl.ds(pl.multiple_of(rep * ROWS, ROWS), ROWS), :] = final[...]
     down_out[pl.ds(pl.multiple_of((1 - rep) * ROWS, ROWS), ROWS), :] = other_final[...]
@@ -418,8 +413,23 @@
     ):
         for copy in small_copies(kind, axis, src, dst):
             copy.wait_send()
-    for store in stores:
-        store.wait()
+
+
+def in_hbm(array):
+    return pltpu.with_memory_space_constraint(array, pltpu.HBM)
+
+
+def finish(gg, gl, conv, down, norms, gg_o, gl_o, tg_o, tl_o, bg_o, bl_o, down_o, norms_o, sems):
+    moves = (
+        (gg, gg_o), (gl, gl_o), (conv.at[pl.ds(0, 3), :], tg_o), (conv.at[pl.ds(3, 3), :], tl_o),
+        (conv.at[pl.ds(6, 1), :], bg_o), (conv.at[pl.ds(7, 1), :], bl_o),
+        (down, down_o), (norms, norms_o),
+    )
+    copies = [pltpu.make_async_copy(a, b, sems.at[k]) for k, (a, b) in enumerate(moves)]
+    for copy in copies:
+        copy.start()
+    for copy in copies:
+        copy.wait()
 
 
 def local(
@@ -428,22 +438,26 @@
     tokens, width = pre_gate.shape
     columns = out_grad.shape[1]
     any_, vmem = pl.BlockSpec(memory_space=pl.ANY), pl.BlockSpec(memory_space=pltpu.VMEM)
+    hbm = pl.BlockSpec(memory_space=pltpu.HBM)
     dma = pltpu.SemaphoreType.DMA
     shape = jax.ShapeDtypeStruct
-    out = pl.pallas_call(
+    held = pl.pallas_call(
         kernel,
         name="gated_backward",
         out_shape=(
-            shape((tokens, width), BF16), shape((tokens, width), BF16),
-            shape((3, width), F32), shape((3, width), F32),
-            shape((1, width), F32), shape((1, width), F32),
-            shape((BLOCK, width), F32), shape((1, width), F32),
+            pltpu.VMEM((tokens, width), BF16), pltpu.VMEM((tokens, width), BF16),
+            pltpu.VMEM((8, width), F32), pltpu.VMEM((BLOCK, width), F32),
+            pltpu.VMEM((1, width), F32),
         ),
-        in_specs=[any_, any_, vmem, vmem, vmem, vmem, any_, any_],
-        out_specs=(any_, any_, vmem, vmem, vmem, vmem, vmem, vmem),
+        in_specs=[hbm] * 8,
+        out_specs=(vmem,) * 5,
         scratch_shapes=[
             pltpu.VMEM((tokens + 16, width), BF16),
             pltpu.VMEM((tokens + 16, width), BF16),
+            pltpu.VMEM((3, width), F32),
+            pltpu.VMEM((3, width), F32),
+            pltpu.VMEM((1, width), F32),
+            pltpu.VMEM((1, width), F32),
             pltpu.VMEM((tokens, columns), BF16),
             pltpu.VMEM((2, columns, HALF), BF16),
             pltpu.VMEM((tokens, width), BF16),
@@ -451,8 +465,6 @@
             pltpu.VMEM((tokens, width), F32),
             pltpu.VMEM((tokens, width), F32),
             pltpu.VMEM((2, columns, HALF), F32),
-            pltpu.VMEM((tokens, width), BF16),
-            pltpu.VMEM((tokens, width), BF16),
             pltpu.VMEM((len(CHAIN), 128, HALF), BF16),
             pltpu.VMEM((len(CHAIN), 128, HALF), BF16),
             pltpu.VMEM((2, RING, ROWS, HALF), F32),
@@ -466,7 +478,7 @@
             pltpu.VMEM((8, width), F32),
             pltpu.VMEM((RING, 8, width), F32),
             pltpu.VMEM((RING + 1, 8, width), F32),
-            dma((5,)), dma((2,)),
+            dma((9,)),
             dma((len(GATHER),)), dma((len(GATHER),)),
             dma((len(CHAIN),)), dma((len(CHAIN),)),
             dma((2, RING)), dma((2, RING)),
@@ -474,13 +486,31 @@
             dma((1,)), dma((1,)),
         ],
         compiler_params=pltpu.CompilerParams(
-            collective_id=0, has_side_effects=True, vmem_limit_bytes=60 * 2**20
+            collective_id=0, has_side_effects=True, vmem_limit_bytes=40 * 2**20
         ),
     )(
-        pre_gate, pre_linear, taps_gate, taps_linear,
-        bias_gate.reshape(1, -1), bias_linear.reshape(1, -1), down_weight.T, out_grad,
+        *map(
+            in_hbm,
+            (
+                pre_gate, pre_linear, taps_gate, taps_linear, bias_gate.reshape(1, -1),
+                bias_linear.reshape(1, -1), down_weight.T, out_grad,
+            ),
+        )
     )
-    gg, gl, tg, tl, bg, bl, down, norms = out
+    gg, gl, tg, tl, bg, bl, down, norms = pl.pallas_call(
+        finish,
+        name="finish",
+        out_shape=(
+            shape((tokens, width), BF16), shape((tokens, width), BF16),
+            shape((3, width), F32), shape((3, width), F32),
+            shape((1, width), F32), shape((1, width), F32),
+            shape((BLOCK, width), F32), shape((1, width), F32),
+        ),
+        in_specs=[vmem] * 5,
+        out_specs=(any_,) * 8,
+        scratch_shapes=[dma((8,))],
+        compiler_params=pltpu.CompilerParams(vmem_limit_bytes=8 * 2**20),
+    )(*held)
     return gg, gl, tg, tl, bg.reshape(-1), bl.reshape(-1), down.T, norms.reshape(-1)
 
 

time: 71.9 us -> 63.8 us (0.89)
  local copies, waits for them, and re-layouts: 7.77 us -> 0 us
    unnamed x20 -> x0, local copies, waits for them, and re-layouts: 7.77 us -> none
    pallas_call x1 -> x2, Pallas kernels: 63 us -> 63 us  [the longest x1 61.7 us: local(): pl.pallas_call(kernel, name='gated_backward', out_shape=(pltpu.VMEM((toke...]
where the time goes in v2:
time: 63.8 us; the launch traced here: 63.6 us
  Pallas kernels  63 us (99%)
  between operations  0.64 us (1%)
    pallas_call x1, Pallas kernels, local(): pl.pallas_call(kernel, name='gated_backward', out_shape=(pltpu.VMEM((toke...  61.7 us

profile of v2, /device:TPU:6, one launch (start us, length us, event | category | flops | bytes accessed | tf_op | source)
XLA Modules:
  0.0 63.6 jit_solution(283150937633795422)
XLA Ops:
  0.6 61.7 %gated_backward.1 = (bf16[768,512]{1,0:T(8,128)(2,1)S(1)}, bf16[768,512]{1,0:T(8,128)(2,1)S(1)}, f32[8,512]{1,0:T(8,128)S(1)}, f32[64,512]{1,0:T(8,128)S(1)}, f32[1,512]{1,0:T(1,128)S(1)}) custom-call(bf16[768,512]{1,0:T(8,128)(2,1)} %gate_hbm.1, bf16[768,512]{1,0:T(8,128)(2,1)} %linear_hbm.1, f32[3,512]{1,0:T(4,128)} %taps_g_hbm.1, f32[3,512]{1,0:T(4,128)} %taps_l_hbm.1, ...), custom_call_target="tpu_custom_call" | custom-call | tf_op jit(solution)/shard_map/gated_backward/pallas_call | solution.py:444
  62.4 1.3 %finish.1 = (bf16[768,512]{1,0:T(8,128)(2,1)}, bf16[768,512]{1,0:T(8,128)(2,1)}, f32[3,512]{1,0:T(4,128)}, f32[3,512]{1,0:T(4,128)}, f32[1,512]{1,0:T(1,128)}, /...) custom-call(bf16[768,512]{1,0:T(8,128)(2,1)S(1)} %get-tuple-element.21.gg, ...), custom_call_target="tpu_custom_call" | custom-call | tf_op jit(solution)/shard_map/finish/pallas_call | solution.py:500

commit v3 on v2

v3 whole, which is shorter than its diff:
```python
import jax
import jax.numpy as jnp
from jax import lax
from jax.experimental import pallas as pl
from jax.experimental.pallas import tpu as pltpu
from jax.sharding import Mesh
from jax.sharding import PartitionSpec as P

REP_FS = ("rep", "fs_0", "fs_1")
RING = 8
BLOCK = 64
HALF = 256
LANES = 128
ROWS = 32
F32, BF16 = jnp.float32, jnp.bfloat16
FAR_FIRST = (4, 3, 5, 2, 6, 1, 7)


def gather_messages():
    found = []

    def add(half, dz, dy, part, axis, sign, needs):
        found.append((half, dz, dy, part, axis, sign, needs))
        return len(found) - 1

    right = add(0, 0, 0, 0, "z", 1, ())
    left = add(0, 0, 0, 0, "z", -1, ())
    right2 = add(0, -1, 0, 1, "z", 1, (right,))
    left2 = add(0, 1, 0, 2, "z", -1, (left,))
    for j, (dz, needs) in enumerate(
        ((0, ()), (-1, (right,)), (1, (left,)), (2, (right2, left2)))
    ):
        for sign, hops in ((1, 4 - j % 2), (-1, 3 + j % 2)):
            before = needs
            for k in range(hops):
                before = (add(0, dz, -sign * k, 0, "y", sign, before),)
    items = [(0, ())]
    for sign, hops in ((1, 4), (-1, 3)):
        before = ()
        for k in range(hops):
            before = (add(1, 0, -sign * k, 0, "y", sign, before),)
            items.append((-sign * (k + 1), before))
    for i, (dy, needs) in enumerate(items):
        first = add(1, 0, dy, 0, "z", 1, needs)
        other = add(1, 0, dy, 0, "z", -1, needs)
        if i % 2 == 0:
            add(1, -1, dy, 0, "z", 1, (first,))
        else:
            add(1, 1, dy, 0, "z", -1, (other,))
    return found


PARTS = 4


def chain_messages():
    return [
        (half, part, sign, step, hops)
        for half in range(2)
        for part in range(PARTS)
        for sign, hops in ((1, 4 - part % 2), (-1, 3 + part % 2))
        for step in range(hops)
    ]


GATHER = gather_messages()
CHAIN = chain_messages()
CHAIN_AT = {m[:4]: k for k, m in enumerate(CHAIN)}


def chain_ends(half, part):
    return [
        CHAIN_AT[half, part, sign, hops - 1]
        for sign, hops in ((1, 4 - part % 2), (-1, 3 + part % 2))
    ]


RATE, FIRST_HOP, NEXT_HOP, BACKLOG = 44.4, 2.1, 0.8, 1.5


def steps():
    found = {}

    def step(name, time, rank, after=(), needs=(), sends=(), start=0.0):
        found[name] = (time, rank, start, tuple(after), tuple(needs), tuple(sends))

    def to_all(kind, half, axis, size):
        return [
            ((kind, half, shift), axis, 1 if shift < 4 + (half == 0) else -1, size,
             min(shift, RING - shift))
            for shift in FAR_FIRST
        ]

    follow = [1] * len(GATHER)
    for k in reversed(range(len(GATHER))):
        for n in GATHER[k][6]:
            follow[n] = max(follow[n], follow[k] + 1)
    for k, (half, _, _, part, axis, sign, needs) in enumerate(GATHER):
        step(("g", k), 0.04, 0.3 - 0.01 * follow[k], (), [("g", n) for n in needs],
             [(("g", k), axis, sign, 16 if part else 32, 1)], 1.0)
    for half in range(2):
        first, second = ("y", "z") if half == 0 else ("z", "y")
        for i in range(2):
            step(("f", half, i), 0.5, 3 + half, [("f", half, 0)] * i, start=2.0)
        for i in range(4):
            before = [("f", half, 1)] + [("w", half, i - 1)] * (i > 0)
            step(("w", half, i), 0.38, 2.5 + half, before, start=2.5)
        for k, (h, part, sign, at, hops) in enumerate(CHAIN):
            if h == half:
                ready = ("w", half, part if half == 0 else 3)
                step(("c", k), 0.07, 0.6 - 0.01 * (hops - at) - 0.1 * half, [ready],
                     [("c", k - 1)] * (at > 0), [(("c", k), first, sign, 128 // PARTS, 1)])
        ends = [("c", k) for part in range(PARTS) for k in chain_ends(half, part)]
        step(("ce", half), 0.25, 0.2, [("w", half, 3)], ends)
        step(("xs", half), 0.02, 0.1, [("ce", 0), ("ce", 1)], (), to_all("x", half, second, 16))
        step(("xe", half), 0.15, 0.1, [("xs", half)], [("x", half, n) for n in FAR_FIRST],
             to_all("ny", half, "y", 1))
        step(("ne", half), 0.1, 0.1, [("xe", half)], [("ny", half, n) for n in FAR_FIRST],
             to_all("nz", half, "z", 1))
        step(("no", half), 0.1, 0.1, [("ne", half)], [("nz", half, n) for n in FAR_FIRST])
        step(("ss", half), 0.02, 6, [("ne", half)], (),
             [(("s", half), "z", 1 if half else -1, 32, 4)])
        step(("so", half), 0.05, 6, [("ss", half)], [("s", half)])
        every = [("g", k) for k, m in enumerate(GATHER) if m[0] == half]
        for i in range(3):
            before = [("h", half, i - 1)] if i else every
            step(("h", half, i), 0.3, 5, before, () if i else every)
            step(("b", half, i), 0.45, 5, [("h", half, i)] + [("b", half, i - 1)] * (i > 0), (),
                 to_all("vy", half, "y", 8) if i == 2 else ())
        step(("ve", half), 0.1, 0.2, [("b", half, 2), ("ce", 1)],
             [("vy", half, n) for n in FAR_FIRST], to_all("vz", half, "z", 8))
        step(("vo", half), 0.1, 0.2, [("ve", half)], [("vz", half, n) for n in FAR_FIRST])
    return found


def planned():
    left = steps()
    clock, order, done, arrival = 0.0, [], set(), {}
    free = {(axis, sign): 0.0 for axis in "yz" for sign in (1, -1)}
    while left:
        choices = []
        for name, (_, rank, start, after, needs, sends) in left.items():
            if all(n in done for n in after) and all(n in arrival for n in needs):
                at = max([start] + [arrival[n] for n in needs])
                if name[0] == "g":
                    at = max(at, free[sends[0][1:3]] - BACKLOG)
                choices.append((max(at - clock, 0.0), rank, at, name))
        wait, _, _, name = min(choices)
        time, sends = left[name][0], left[name][5]
        del left[name]
        clock += wait + time
        order.append(name)
        done.add(name)
        for message, axis, sign, size, hops in sends:
            gone = max(clock, free[axis, sign]) + size * hops / RATE
            free[axis, sign] = gone
            arrival[message] = gone + FIRST_HOP + NEXT_HOP * (hops - 1)
    return order


ORDER = planned()


def kernel(
    gate_hbm, linear_hbm, taps_g_hbm, taps_l_hbm, bias_g_hbm, bias_l_hbm, weight_hbm,
    out_grad_hbm,
    gg, gl, conv_out, down_out, norms_out,
    gate, linear, taps_g, taps_l, bias_g, bias_l, out_grad, weights, hidden, factor_g, factor_l, grad_hidden, partial,
    chain_send, chain_recv, summed, cross_send, cross_recv, final, other_final,
    rows_g, rows_l, after_g, after_l, sums, conv_y, conv_z, norm_y, norm_z,
    load_sem, gather_s, gather_r, chain_s, chain_r, cross_s, cross_r,
    small_s, small_r, swap_s, swap_r,
):
    tokens = gate_hbm.shape[0]
    rep, z_lo, y = lax.axis_index("rep"), lax.axis_index("fs_0"), lax.axis_index("fs_1")
    z = rep * 4 + z_lo

    def along(axis, shift):
        if axis == "y":
            return {"fs_1": lax.rem(y + shift + RING, RING)}
        at = lax.rem(z + shift + RING, RING)
        return {"rep": at // 4, "fs_0": lax.rem(at, 4)}

    def remote(src, dst, send, recv, axis, shift):
        return pltpu.make_async_remote_copy(
            src_ref=src, dst_ref=dst, send_sem=send, recv_sem=recv,
            device_id=along(axis, shift), device_id_type=pl.DeviceIdType.MESH,
        )

    barrier = pltpu.get_barrier_semaphore()
    for axis in ("y", "z"):
        for shift in (1, -1):
            pl.semaphore_signal(
                barrier, inc=1, device_id=along(axis, shift),
                device_id_type=pl.DeviceIdType.MESH,
            )

    own_row = pl.multiple_of((z_lo * 8 + y) * BLOCK, BLOCK)
    loads = [
        pltpu.make_async_copy(
            weight_hbm.at[:, pl.ds(h * HALF, HALF)],
            weights.at[h, pl.ds(own_row, BLOCK), :],
            load_sem.at[h],
        )
        for h in range(2)
    ]
    loads += [
        pltpu.make_async_copy(gate_hbm, gate, load_sem.at[2]),
        pltpu.make_async_copy(linear_hbm, linear, load_sem.at[3]),
        pltpu.make_async_copy(taps_g_hbm, taps_g, load_sem.at[5]),
        pltpu.make_async_copy(taps_l_hbm, taps_l, load_sem.at[6]),
        pltpu.make_async_copy(bias_g_hbm, bias_g, load_sem.at[7]),
        pltpu.make_async_copy(bias_l_hbm, bias_l, load_sem.at[8]),
        pltpu.make_async_copy(out_grad_hbm, out_grad, load_sem.at[4]),
    ]
    for load in loads:
        load.start()
    strips = rows_g.shape[0]
    for ref in (rows_g, rows_l):
        ref[:, 0:8, :] = jnp.zeros((strips, 8, LANES), F32)
    for ref in (after_g, after_l):
        ref[:, tokens : tokens + 8, :] = jnp.zeros((strips, 8, LANES), F32)

    def gather_copy(k):
        half, dz, dy, part, axis, sign, _ = GATHER[k]
        at = lax.rem(z_lo + dz + 4, 4) * 8 + lax.rem(y + dy + RING, RING)
        start, size = at * BLOCK, BLOCK
        if part:
            start, size = start + (part - 1) * 32, 32
        block = weights.at[half, pl.ds(pl.multiple_of(start, size), size), :]
        return remote(block, block, gather_s.at[k], gather_r.at[k], axis, sign)

    STEP = 64

    def strips_of(half):
        return [(n, slice(n * LANES, (n + 1) * LANES)) for n in (2 * half, 2 * half + 1)]

    def forward(half, seg):
        blocks = tokens // STEP // 2
        for n, lanes in strips_of(half):
            tg, tl = taps_g[0:3, lanes], taps_l[0:3, lanes]
            bg, bl = bias_g[0:1, lanes], bias_l[0:1, lanes]

            def convolve(source, rows, row, taps, bias):
                last = source[pl.ds(row, STEP), lanes].astype(F32)
                rows[n, pl.ds(row + 8, STEP), :] = last
                return (
                    taps[0:1] * rows[n, pl.ds(row + 6, STEP), :]
                    + taps[1:2] * rows[n, pl.ds(row + 7, STEP), :]
                    + taps[2:3] * last
                    + bias
                )

            def body(i, carry):
                row = pl.multiple_of(i * STEP, STEP)
                gate_pre = convolve(gate, rows_g, row, tg, bg)
                linear_pre = convolve(linear, rows_l, row, tl, bl)
                sigma = 1.0 / (1.0 + jnp.exp(-gate_pre))
                silu = gate_pre * sigma
                hidden[pl.ds(row, STEP), lanes] = (silu * linear_pre).astype(BF16)
                factor_g[pl.ds(row, STEP), lanes] = (
                    linear_pre * sigma * (1.0 + gate_pre * (1.0 - sigma))
                )
                factor_l[pl.ds(row, STEP), lanes] = silu
                return carry

            lax.fori_loop(seg * blocks, (seg + 1) * blocks, body, 0)

    def weight_grad(half, i):
        lanes = slice(half * HALF, (half + 1) * HALF)
        partial[half, i * 512 : (i + 1) * 512, :] = lax.dot_general(
            out_grad[:, i * 512 : (i + 1) * 512], hidden[:, lanes],
            (((0,), (0,)), ((), ())), preferred_element_type=F32,
        )

    def hidden_grad(half, i):
        at, size = (2 - i) * (tokens // 3), tokens // 3
        grad_hidden[at : at + size, half * HALF : (half + 1) * HALF] = jnp.dot(
            out_grad[at : at + size, :], weights[half], preferred_element_type=F32
        )

    def fold(v):
        return jnp.sum(v.reshape(STEP // 8, 8, LANES), axis=0)

    def backward(half, seg):
        blocks = tokens // STEP // 3
        for n, lanes in strips_of(half):
            tg, tl = taps_g[0:3, lanes], taps_l[0:3, lanes]

            def back(v, after, row, taps):
                after[n, pl.ds(row, STEP), :] = v
                return (
                    taps[0:1] * after[n, pl.ds(row + 2, STEP), :]
                    + taps[1:2] * after[n, pl.ds(row + 1, STEP), :]
                    + taps[2:3] * v
                )

            def body(i, totals):
                row = pl.multiple_of((tokens // STEP - 1 - i) * STEP, STEP)
                grad = grad_hidden[pl.ds(row, STEP), lanes]
                dg = grad * factor_g[pl.ds(row, STEP), lanes]
                dl = grad * factor_l[pl.ds(row, STEP), lanes]
                gg[pl.ds(row, STEP), lanes] = back(dg, after_g, row, tg).astype(BF16)
                gl[pl.ds(row, STEP), lanes] = back(dl, after_l, row, tl).astype(BF16)
                terms = [dg * rows_g[n, pl.ds(row + 6 + j, STEP), :] for j in range(3)]
                terms += [dl * rows_l[n, pl.ds(row + 6 + j, STEP), :] for j in range(3)]
                terms += [dg, dl]
                return tuple(total + fold(term) for total, term in zip(totals, terms))

            if seg == 0:
                totals = (jnp.zeros((8, LANES), F32),) * 8
            else:
                totals = tuple(sums[j, :, lanes] for j in range(8))
            totals = lax.fori_loop(seg * blocks, (seg + 1) * blocks, body, totals)
            for j, total in enumerate(totals):
                sums[j, :, lanes] = total
        if seg == 2:
            for n, lanes in strips_of(half):
                for j in range(8):
                    total = jnp.sum(sums[j, :, lanes], axis=0, keepdims=True)
                    at = (n - 2 * half) * LANES
                    conv_y[half, RING, j : j + 1, at : at + LANES] = total
            small_start(0, half, "y", conv_y)

    def first_axis(half):
        return ("y", y) if half == 0 else ("z", z)

    def pieces(half, to, part):
        if half == 0:
            return [(part * 512 + to * 64, 64)]
        return [
            (lax.rem(to, 4) * 512 + (2 * part + q) * 64 + (to // 4) * 32, 32) for q in range(2)
        ]

    def chain_copy(k):
        half, part, sign, step, hops = CHAIN[k]
        return remote(
            chain_send.at[k], chain_recv.at[k], chain_s.at[k], chain_r.at[k],
            first_axis(half)[0], sign,
        )

    def chain_step(k):
        half, part, sign, step, hops = CHAIN[k]
        to = lax.rem(first_axis(half)[1] + sign * (hops - step) + RING, RING)
        at = 0
        for row, size in pieces(half, to, part):
            value = partial[half, pl.ds(pl.multiple_of(row, size), size), :]
            if step:
                value = value + chain_recv[k - 1, at : at + size, :].astype(F32)
            chain_send[k, at : at + size, :] = value.astype(BF16)
            at += size
        chain_copy(k).start()

    def chain_end(half):
        for part in range(PARTS):
            at = 0
            for row, size in pieces(half, first_axis(half)[1], part):
                value = partial[half, pl.ds(pl.multiple_of(row, size), size), :]
                for k in chain_ends(half, part):
                    value = value + chain_recv[k, at : at + size, :].astype(F32)
                for sub in range(size // ROWS):
                    slot = (part * BLOCK + at) // ROWS + sub
                    piece = value[sub * ROWS : (sub + 1) * ROWS]
                    summed[half, slot] = piece
                    cross_send[half, slot] = piece.astype(BF16)
                at += size

    def slot_of(half, at):
        return lax.rem(at, 4) * 2 + at // 4 if half == 0 else at

    def cross_copy(half, shift):
        axis, here = ("z", z) if half == 0 else ("y", y)
        slot = slot_of(half, lax.rem(here + shift, RING))
        return remote(
            cross_send.at[half, slot], cross_recv.at[half, shift],
            cross_s.at[half, shift], cross_r.at[half, shift], axis, shift,
        )

    def cross_start(half):
        for shift in FAR_FIRST:
            cross_copy(half, shift).start()

    def cross_end(half):
        here = z if half == 0 else y
        value = summed[half, slot_of(half, here)]
        for shift in FAR_FIRST:
            value = value + cross_recv[half, shift].astype(F32)
        final[half] = value
        norm_y[half, RING, 0:1, :] = jnp.sum(value * value, axis=0, keepdims=True)
        small_start(1, half, "y", norm_y)

    def swap_copy(half):
        return remote(
            final.at[half], other_final.at[half], swap_s.at[half], swap_r.at[half], "z", 4
        )

    SMALL = {"vy": (0, "y", conv_y), "vz": (0, "z", conv_z),
             "ny": (1, "y", norm_y), "nz": (1, "z", norm_z)}

    def small_copy(kind, half, axis, ref, shift):
        here = y if axis == "y" else z
        sem = ((kind * 2 + (axis == "z")) * 2 + half) * RING + shift
        size = 1 if kind else 8
        return remote(
            ref.at[half, RING, pl.ds(0, size), :], ref.at[half, here, pl.ds(0, size), :],
            small_s.at[sem], small_r.at[sem], axis, shift,
        )

    def small_start(kind, half, axis, ref):
        here = y if axis == "y" else z
        size = 1 if kind else 8
        for shift in FAR_FIRST:
            small_copy(kind, half, axis, ref, shift).start()
        ref[half, here, 0:size, :] = ref[half, RING, 0:size, :]

    def small_total(kind, half, ref):
        size = 1 if kind else 8
        value = ref[half, 0, 0:size, :]
        for k in range(1, RING):
            value = value + ref[half, k, 0:size, :]
        return value

    def small_on(kind, half, source, ref):
        ref[half, RING, 0 : 1 if kind else 8, :] = small_total(kind, half, source)
        small_start(kind, half, "z", ref)

    def conv_done(half):
        conv_out[:, half * HALF : (half + 1) * HALF] = small_total(0, half, conv_z)

    def norm_done(half):
        norms_out[:, half * HALF : (half + 1) * HALF] = small_total(1, half, norm_z)

    def swap_done(half):
        lanes = slice(half * HALF, (half + 1) * HALF)
        here, there = (pl.ds(pl.multiple_of(r * ROWS, ROWS), ROWS) for r in (rep, 1 - rep))
        down_out[here, lanes] = final[half]
        down_out[there, lanes] = other_final[half]

    def message(name):
        if name[0] == "g":
            return gather_copy(name[1])
        if name[0] == "c":
            return chain_copy(name[1])
        if name[0] == "x":
            return cross_copy(*name[1:])
        if name[0] == "s":
            return swap_copy(name[1])
        kind, axis, ref = SMALL[name[0]]
        return small_copy(kind, name[1], axis, ref, name[2])

    run = {
        "g": lambda k: gather_copy(k).start(),
        "f": forward, "w": weight_grad, "h": hidden_grad, "b": backward,
        "c": chain_step, "ce": chain_end, "xs": cross_start, "xe": cross_end,
        "ss": lambda half: swap_copy(half).start(), "so": swap_done,
        "ne": lambda half: small_on(1, half, norm_y, norm_z), "no": norm_done,
        "ve": lambda half: small_on(0, half, conv_y, conv_z), "vo": conv_done,
    }

    loads[0].wait()
    loads[1].wait()
    pl.semaphore_wait(barrier, 4)
    loaded = 2
    seen = []
    plan = steps()
    for name in ORDER:
        want = {"f": 8, "w": 9}.get(name[0], 0)
        for load in loads[loaded:want]:
            load.wait()
        loaded = max(loaded, want)
        for needed in plan[name][4]:
            if needed not in seen:
                message(needed).wait_recv()
                seen.append(needed)
        run[name[0]](*name[1:])
    for name in seen:
        message(name).wait_send()


def in_hbm(array):
    return pltpu.with_memory_space_constraint(array, pltpu.HBM)


def finish(gg, gl, conv, down, norms, gg_o, gl_o, tg_o, tl_o, bg_o, bl_o, down_o, norms_o, sems):
    moves = (
        (gg, gg_o), (gl, gl_o), (conv.at[pl.ds(0, 3), :], tg_o), (conv.at[pl.ds(3, 3), :], tl_o),
        (conv.at[pl.ds(6, 1), :], bg_o), (conv.at[pl.ds(7, 1), :], bl_o),
        (down, down_o), (norms, norms_o),
    )
    copies = [pltpu.make_async_copy(a, b, sems.at[k]) for k, (a, b) in enumerate(moves)]
    for copy in copies:
        copy.start()
    for copy in copies:
        copy.wait()


def local(
    pre_gate, pre_linear, taps_gate, taps_linear, bias_gate, bias_linear, down_weight, out_grad
):
    tokens, width = pre_gate.shape
    columns = out_grad.shape[1]
    any_, vmem = pl.BlockSpec(memory_space=pl.ANY), pl.BlockSpec(memory_space=pltpu.VMEM)
    hbm = pl.BlockSpec(memory_space=pltpu.HBM)
    dma = pltpu.SemaphoreType.DMA
    shape = jax.ShapeDtypeStruct
    held = pl.pallas_call(
        kernel,
        name="gated_backward",
        out_shape=(
            pltpu.VMEM((tokens, width), BF16), pltpu.VMEM((tokens, width), BF16),
            pltpu.VMEM((8, width), F32), pltpu.VMEM((BLOCK, width), F32),
            pltpu.VMEM((1, width), F32),
        ),
        in_specs=[hbm] * 8,
        out_specs=(vmem,) * 5,
        scratch_shapes=[
            pltpu.VMEM((tokens, width), BF16),
            pltpu.VMEM((tokens, width), BF16),
            pltpu.VMEM((3, width), F32),
            pltpu.VMEM((3, width), F32),
            pltpu.VMEM((1, width), F32),
            pltpu.VMEM((1, width), F32),
            pltpu.VMEM((tokens, columns), BF16),
            pltpu.VMEM((2, columns, HALF), BF16),
            pltpu.VMEM((tokens, width), BF16),
            pltpu.VMEM((tokens, width), F32),
            pltpu.VMEM((tokens, width), F32),
            pltpu.VMEM((tokens, width), F32),
            pltpu.VMEM((2, columns, HALF), F32),
            pltpu.VMEM((len(CHAIN), BLOCK, HALF), BF16),
            pltpu.VMEM((len(CHAIN), BLOCK, HALF), BF16),
            pltpu.VMEM((2, RING, ROWS, HALF), F32),
            pltpu.VMEM((2, RING, ROWS, HALF), BF16),
            pltpu.VMEM((2, RING, ROWS, HALF), BF16),
            pltpu.VMEM((2, ROWS, HALF), F32),
            pltpu.VMEM((2, ROWS, HALF), F32),
            pltpu.VMEM((width // LANES, tokens + 8, LANES), F32),
            pltpu.VMEM((width // LANES, tokens + 8, LANES), F32),
            pltpu.VMEM((width // LANES, tokens + 8, LANES), F32),
            pltpu.VMEM((width // LANES, tokens + 8, LANES), F32),
            pltpu.VMEM((8, 8, width), F32),
            pltpu.VMEM((2, RING + 1, 8, HALF), F32),
            pltpu.VMEM((2, RING + 1, 8, HALF), F32),
            pltpu.VMEM((2, RING + 1, 8, HALF), F32),
            pltpu.VMEM((2, RING + 1, 8, HALF), F32),
            dma((9,)),
            dma((len(GATHER),)), dma((len(GATHER),)),
            dma((len(CHAIN),)), dma((len(CHAIN),)),
            dma((2, RING)), dma((2, RING)),
            dma((8 * RING,)), dma((8 * RING,)),
            dma((2,)), dma((2,)),
        ],
        compiler_params=pltpu.CompilerParams(
            collective_id=0, has_side_effects=True, vmem_limit_bytes=40 * 2**20
        ),
    )(
        *map(
            in_hbm,
            (
                pre_gate, pre_linear, taps_gate, taps_linear, bias_gate.reshape(1, -1),
                bias_linear.reshape(1, -1), down_weight.T, out_grad,
            ),
        )
    )
    gg, gl, tg, tl, bg, bl, down, norms = pl.pallas_call(
        finish,
        name="finish",
        out_shape=(
            shape((tokens, width), BF16), shape((tokens, width), BF16),
            shape((3, width), F32), shape((3, width), F32),
            shape((1, width), F32), shape((1, width), F32),
            shape((BLOCK, width), F32), shape((1, width), F32),
        ),
        in_specs=[vmem] * 5,
        out_specs=(any_,) * 8,
        scratch_shapes=[dma((8,))],
        compiler_params=pltpu.CompilerParams(vmem_limit_bytes=8 * 2**20),
    )(*held)
    return gg, gl, tg, tl, bg.reshape(-1), bl.reshape(-1), down.T, norms.reshape(-1)


def solution(mesh):
    split = Mesh(
        mesh.devices.reshape(mesh.shape["rep"], 4, 8, mesh.shape["tp"]),
        ("rep", "fs_0", "fs_1", "tp"),
    )
    fs = ("fs_0", "fs_1")
    in_specs = (
        P(REP_FS, "tp"), P(REP_FS, "tp"), P(None, "tp"), P(None, "tp"),
        P("tp"), P("tp"), P("tp", fs), P(REP_FS, None),
    )
    out_specs = (
        P(REP_FS, "tp"), P(REP_FS, "tp"), P(None, "tp"), P(None, "tp"),
        P("tp"), P("tp"), P("tp", fs), P("tp"),
    )
    return jax.shard_map(local, mesh=split, in_specs=in_specs, out_specs=out_specs, check_vma=False)
```

time: 63.8 us -> 60.8 us (0.953)
  Pallas kernels: 63 us -> 60.1 us
    pallas_call x1, Pallas kernels: 61.7 us -> 58.8 us  [local(): pl.pallas_call(kernel, name='gated_backward', out_shape=(pltpu.VMEM((toke...]
where the time goes in v3:
time: 60.8 us; the launch traced here: 60.7 us
  Pallas kernels  60.1 us (99%)
  between operations  0.64 us (1%)
    pallas_call x1, Pallas kernels, local(): pl.pallas_call(kernel, name='gated_backward', out_shape=(pltpu.VMEM((toke...  58.8 us
    pallas_call x1, Pallas kernels, local(): pl.pallas_call(finish, name='finish', out_shape=(shape((tokens, width), B...  1.26 us

profile of v3, /device:TPU:6, one launch (start us, length us, event | category | flops | bytes accessed | tf_op | source)
XLA Modules:
  0.0 60.7 jit_solution(3420970785605131741)
XLA Ops:
  0.6 58.8 %gated_backward.1 = (bf16[768,512]{1,0:T(8,128)(2,1)S(1)}, bf16[768,512]{1,0:T(8,128)(2,1)S(1)}, f32[8,512]{1,0:T(8,128)S(1)}, f32[64,512]{1,0:T(8,128)S(1)}, f32[1,512]{1,0:T(1,128)S(1)}) custom-call(bf16[768,512]{1,0:T(8,128)(2,1)} %gate_hbm.1, bf16[768,512]{1,0:T(8,128)(2,1)} %linear_hbm.1, f32[3,512]{1,0:T(4,128)} %taps_g_hbm.1, f32[3,512]{1,0:T(4,128)} %taps_l_hbm.1, ...), custom_call_target="tpu_custom_call" | custom-call | tf_op jit(solution)/shard_map/gated_backward/pallas_call | solution.py:506
  59.5 1.3 %finish.1 = (bf16[768,512]{1,0:T(8,128)(2,1)}, bf16[768,512]{1,0:T(8,128)(2,1)}, f32[3,512]{1,0:T(4,128)}, f32[3,512]{1,0:T(4,128)}, f32[1,512]{1,0:T(1,128)}, /...) custom-call(bf16[768,512]{1,0:T(8,128)(2,1)S(1)} %get-tuple-element.21.gg, ...), custom_call_target="tpu_custom_call" | custom-call | tf_op jit(solution)/shard_map/finish/pallas_call | solution.py:565

commit v4 on v3

--- a/solution.py
+++ b/solution.py
@@ -51,6 +51,8 @@
 
 
 PARTS = 4
+Z_OFF = (0, 1, 3, 2)
+Y_OFF = ((4, 0), (3, 5), (2, 6), (1, 7))
 
 
 def chain_messages():
@@ -75,7 +77,13 @@
     ]
 
 
-RATE, FIRST_HOP, NEXT_HOP, BACKLOG = 44.4, 2.1, 0.8, 1.5
+def cross_shifts(half, part):
+    if half == 1:
+        return [n for n in Y_OFF[part] if n]
+    return [n for n in FAR_FIRST if n % 4 == Z_OFF[part]]
+
+
+RATE, FIRST_HOP, NEXT_HOP = 44.4, 2.8, 0.8
 
 
 def steps():
@@ -91,6 +99,8 @@
             for shift in FAR_FIRST
         ]
 
+    for i in range(4):
+        step(("w", i), 0.55, 2.5, [("w", i - 1)] if i else [("f", 1, 0), ("f", 1, 1)], start=2.5)
     follow = [1] * len(GATHER)
     for k in reversed(range(len(GATHER))):
         for n in GATHER[k][6]:
@@ -101,19 +111,19 @@
     for half in range(2):
         first, second = ("y", "z") if half == 0 else ("z", "y")
         for i in range(2):
-            step(("f", half, i), 0.5, 3 + half, [("f", half, 0)] * i, start=2.0)
-        for i in range(4):
-            before = [("f", half, 1)] + [("w", half, i - 1)] * (i > 0)
-            step(("w", half, i), 0.38, 2.5 + half, before, start=2.5)
+            step(("f", i, half), 0.5, 3 + i, [("f", 0, half)] * i, start=1.6 + 0.4 * i)
         for k, (h, part, sign, at, hops) in enumerate(CHAIN):
             if h == half:
-                ready = ("w", half, part if half == 0 else 3)
+                ready = ("w", part if half == 0 else Z_OFF.index(sign * (hops - at) % 4))
                 step(("c", k), 0.07, 0.6 - 0.01 * (hops - at) - 0.1 * half, [ready],
                      [("c", k - 1)] * (at > 0), [(("c", k), first, sign, 128 // PARTS, 1)])
-        ends = [("c", k) for part in range(PARTS) for k in chain_ends(half, part)]
-        step(("ce", half), 0.25, 0.2, [("w", half, 3)], ends)
-        step(("xs", half), 0.02, 0.1, [("ce", 0), ("ce", 1)], (), to_all("x", half, second, 16))
-        step(("xe", half), 0.15, 0.1, [("xs", half)], [("x", half, n) for n in FAR_FIRST],
+        for part in range(PARTS):
+            step(("ce", half, part), 0.07, 0.2, [("w", 3)],
+                 [("c", k) for k in chain_ends(half, part)])
+            step(("xs", half, part), 0.02, 0.1, [("ce", half, part), ("ce", 1 - half, 0)], (),
+                 [m for m in to_all("x", half, second, 16) if m[0][2] in cross_shifts(half, part)])
+        step(("xe", half), 0.15, 0.1, [("xs", half, part) for part in range(PARTS)],
+             [("x", half, n) for n in FAR_FIRST],
              to_all("ny", half, "y", 1))
         step(("ne", half), 0.1, 0.1, [("xe", half)], [("ny", half, n) for n in FAR_FIRST],
              to_all("nz", half, "z", 1))
@@ -125,40 +135,38 @@
         for i in range(3):
             before = [("h", half, i - 1)] if i else every
             step(("h", half, i), 0.3, 5, before, () if i else every)
-            step(("b", half, i), 0.45, 5, [("h", half, i)] + [("b", half, i - 1)] * (i > 0), (),
+            step(("b", half, i), 0.4, 5, [("h", half, i)] + [("b", half, i - 1)] * (i > 0), (),
                  to_all("vy", half, "y", 8) if i == 2 else ())
-        step(("ve", half), 0.1, 0.2, [("b", half, 2), ("ce", 1)],
+        step(("ve", half), 0.1, 0.2, [("b", half, 2), ("ce", 1, 0)],
              [("vy", half, n) for n in FAR_FIRST], to_all("vz", half, "z", 8))
         step(("vo", half), 0.1, 0.2, [("ve", half)], [("vz", half, n) for n in FAR_FIRST])
     return found
 
 
-def planned():
-    left = steps()
-    clock, order, done, arrival = 0.0, [], set(), {}
-    free = {(axis, sign): 0.0 for axis in "yz" for sign in (1, -1)}
-    while left:
-        choices = []
-        for name, (_, rank, start, after, needs, sends) in left.items():
-            if all(n in done for n in after) and all(n in arrival for n in needs):
-                at = max([start] + [arrival[n] for n in needs])
-                if name[0] == "g":
-                    at = max(at, free[sends[0][1:3]] - BACKLOG)
-                choices.append((max(at - clock, 0.0), rank, at, name))
-        wait, _, _, name = min(choices)
-        time, sends = left[name][0], left[name][5]
-        del left[name]
-        clock += wait + time
-        order.append(name)
-        done.add(name)
-        for message, axis, sign, size, hops in sends:
-            gone = max(clock, free[axis, sign]) + size * hops / RATE
-            free[axis, sign] = gone
-            arrival[message] = gone + FIRST_HOP + NEXT_HOP * (hops - 1)
-    return order
-
-
-ORDER = planned()
+ORDER = (
+    ("g", 32), ("g", 0), ("g", 4), ("g", 8), ("g", 40), ("g", 36), ("g", 1), ("g", 39),
+    ("f", 0, 0), ("f", 1, 0), ("f", 0, 1), ("f", 1, 1), ("w", 0), ("c", 4), ("c", 38), ("g", 43),
+    ("c", 52), ("g", 11), ("g", 33), ("c", 0), ("g", 14), ("g", 9), ("g", 42), ("g", 2),
+    ("c", 28), ("c", 42), ("w", 1), ("g", 3), ("g", 37), ("c", 32), ("c", 46), ("g", 18),
+    ("c", 7), ("c", 10), ("w", 2), ("g", 41), ("c", 49), ("c", 18), ("c", 14), ("c", 35),
+    ("w", 3), ("g", 55), ("c", 5), ("c", 24), ("c", 39), ("c", 21), ("g", 54), ("g", 34),
+    ("g", 46), ("g", 10), ("c", 53), ("g", 45), ("c", 29), ("c", 1), ("g", 38), ("c", 43),
+    ("g", 25), ("c", 33), ("c", 11), ("c", 8), ("c", 47), ("c", 19), ("c", 50), ("c", 15),
+    ("g", 44), ("c", 6), ("c", 36), ("c", 22), ("c", 40), ("c", 25), ("g", 57), ("g", 35),
+    ("g", 58), ("g", 28), ("g", 48), ("c", 2), ("c", 54), ("g", 22), ("c", 30), ("g", 19),
+    ("c", 34), ("c", 12), ("c", 44), ("c", 9), ("c", 48), ("c", 20), ("c", 51), ("c", 16),
+    ("g", 61), ("g", 15), ("c", 37), ("c", 23), ("c", 41), ("c", 26), ("g", 59), ("g", 5),
+    ("g", 52), ("g", 29), ("g", 51), ("c", 3), ("c", 55), ("g", 23), ("c", 31), ("g", 20),
+    ("g", 49), ("c", 13), ("c", 45), ("g", 26), ("g", 56), ("g", 60), ("c", 17), ("g", 62),
+    ("g", 16), ("g", 47), ("g", 12), ("ce", 1, 1), ("c", 27), ("g", 6), ("g", 30), ("g", 53),
+    ("ce", 0, 0), ("xs", 1, 1), ("ce", 1, 3), ("xs", 1, 3), ("ce", 1, 0), ("xs", 0, 0),
+    ("xs", 1, 0), ("g", 50), ("ce", 0, 1), ("xs", 0, 1), ("ce", 1, 2), ("xs", 1, 2), ("ce", 0, 2),
+    ("g", 27), ("xs", 0, 2), ("ce", 0, 3), ("xs", 0, 3), ("g", 13), ("g", 31), ("g", 7),
+    ("h", 1, 0), ("g", 17), ("h", 1, 1), ("g", 21), ("h", 1, 2), ("g", 24), ("b", 1, 0),
+    ("b", 1, 1), ("b", 1, 2), ("xe", 0), ("xe", 1), ("h", 0, 0), ("b", 0, 0), ("h", 0, 1),
+    ("h", 0, 2), ("b", 0, 1), ("b", 0, 2), ("ve", 1), ("ne", 0), ("ss", 0), ("ne", 1), ("ss", 1),
+    ("ve", 0), ("vo", 1), ("no", 0), ("so", 1), ("so", 0), ("no", 1), ("vo", 0),
+)
 
 
 def kernel(
@@ -205,12 +213,30 @@
         for h in range(2)
     ]
     loads += [
-        pltpu.make_async_copy(gate_hbm, gate, load_sem.at[2]),
-        pltpu.make_async_copy(linear_hbm, linear, load_sem.at[3]),
+        pltpu.make_async_copy(source.at[rows, :], to.at[rows, :], load_sem.at[k])
+        for k, (source, to, rows) in enumerate(
+            (
+                (gate_hbm, gate, pl.ds(0, tokens // 2)),
+                (linear_hbm, linear, pl.ds(0, tokens // 2)),
+            ),
+            2,
+        )
+    ]
+    loads += [
         pltpu.make_async_copy(taps_g_hbm, taps_g, load_sem.at[5]),
         pltpu.make_async_copy(taps_l_hbm, taps_l, load_sem.at[6]),
         pltpu.make_async_copy(bias_g_hbm, bias_g, load_sem.at[7]),
         pltpu.make_async_copy(bias_l_hbm, bias_l, load_sem.at[8]),
+        pltpu.make_async_copy(
+            gate_hbm.at[pl.ds(tokens // 2, tokens // 2), :],
+            gate.at[pl.ds(tokens // 2, tokens // 2), :],
+            load_sem.at[9],
+        ),
+        pltpu.make_async_copy(
+            linear_hbm.at[pl.ds(tokens // 2, tokens // 2), :],
+            linear.at[pl.ds(tokens // 2, tokens // 2), :],
+            load_sem.at[10],
+        ),
         pltpu.make_async_copy(out_grad_hbm, out_grad, load_sem.at[4]),
     ]
     for load in loads:
@@ -235,7 +261,7 @@
     def strips_of(half):
         return [(n, slice(n * LANES, (n + 1) * LANES)) for n in (2 * half, 2 * half + 1)]
 
-    def forward(half, seg):
+    def forward(seg, half):
         blocks = tokens // STEP // 2
         for n, lanes in strips_of(half):
             tg, tl = taps_g[0:3, lanes], taps_l[0:3, lanes]
@@ -266,12 +292,13 @@
 
             lax.fori_loop(seg * blocks, (seg + 1) * blocks, body, 0)
 
-    def weight_grad(half, i):
-        lanes = slice(half * HALF, (half + 1) * HALF)
-        partial[half, i * 512 : (i + 1) * 512, :] = lax.dot_general(
-            out_grad[:, i * 512 : (i + 1) * 512], hidden[:, lanes],
-            (((0,), (0,)), ((), ())), preferred_element_type=F32,
-        )
+    def weight_grad(i):
+        rows = pl.ds(pl.multiple_of(lax.rem(z_lo + Z_OFF[i], 4) * 512, 512), 512)
+        product = lax.dot_general(
+            out_grad[:, rows], hidden[...], (((0,), (0,)), ((), ())), preferred_element_type=F32
+        )
+        partial[0, rows, :] = product[:, :HALF]
+        partial[1, rows, :] = product[:, HALF:]
 
     def hidden_grad(half, i):
         at, size = (2 - i) * (tokens // 3), tokens // 3
@@ -327,9 +354,10 @@
 
     def pieces(half, to, part):
         if half == 0:
-            return [(part * 512 + to * 64, 64)]
+            return [(lax.rem(z_lo + Z_OFF[part], 4) * 512 + to * 64, 64)]
         return [
-            (lax.rem(to, 4) * 512 + (2 * part + q) * 64 + (to // 4) * 32, 32) for q in range(2)
+            (lax.rem(to, 4) * 512 + lax.rem(y + n, RING) * 64 + (to // 4) * 32, 32)
+            for n in Y_OFF[part]
         ]
 
     def chain_copy(k):
@@ -351,38 +379,37 @@
             at += size
         chain_copy(k).start()
 
-    def chain_end(half):
-        for part in range(PARTS):
-            at = 0
-            for row, size in pieces(half, first_axis(half)[1], part):
-                value = partial[half, pl.ds(pl.multiple_of(row, size), size), :]
-                for k in chain_ends(half, part):
-                    value = value + chain_recv[k, at : at + size, :].astype(F32)
-                for sub in range(size // ROWS):
-                    slot = (part * BLOCK + at) // ROWS + sub
-                    piece = value[sub * ROWS : (sub + 1) * ROWS]
-                    summed[half, slot] = piece
-                    cross_send[half, slot] = piece.astype(BF16)
-                at += size
-
-    def slot_of(half, at):
-        return lax.rem(at, 4) * 2 + at // 4 if half == 0 else at
+    def chain_end(half, part):
+        at = 0
+        for row, size in pieces(half, first_axis(half)[1], part):
+            value = partial[half, pl.ds(pl.multiple_of(row, size), size), :]
+            for k in chain_ends(half, part):
+                value = value + chain_recv[k, at : at + size, :].astype(F32)
+            for sub in range(size // ROWS):
+                slot = (part * BLOCK + at) // ROWS + sub
+                piece = value[sub * ROWS : (sub + 1) * ROWS]
+                summed[half, slot] = piece
+                cross_send[half, slot] = piece.astype(BF16)
+            at += size
+
+    def slot_of(half, shift):
+        if half == 0:
+            return 2 * Z_OFF.index(shift % 4) + lax.rem(z + shift, RING) // 4
+        return [n for part in Y_OFF for n in part].index(shift)
 
     def cross_copy(half, shift):
-        axis, here = ("z", z) if half == 0 else ("y", y)
-        slot = slot_of(half, lax.rem(here + shift, RING))
+        slot = slot_of(half, shift)
         return remote(
             cross_send.at[half, slot], cross_recv.at[half, shift],
-            cross_s.at[half, shift], cross_r.at[half, shift], axis, shift,
-        )
-
-    def cross_start(half):
-        for shift in FAR_FIRST:
+            cross_s.at[half, shift], cross_r.at[half, shift], "y" if half else "z", shift,
+        )
+
+    def cross_start(half, part):
+        for shift in cross_shifts(half, part):
             cross_copy(half, shift).start()
 
     def cross_end(half):
-        here = z if half == 0 else y
-        value = summed[half, slot_of(half, here)]
+        value = summed[half, slot_of(half, 0)]
         for shift in FAR_FIRST:
             value = value + cross_recv[half, shift].astype(F32)
         final[half] = value
@@ -464,7 +491,7 @@
     seen = []
     plan = steps()
     for name in ORDER:
-        want = {"f": 8, "w": 9}.get(name[0], 0)
+        want = {"f": 8 + 2 * name[1], "w": 11}.get(name[0], 0)
         for load in loads[loaded:want]:
             load.wait()
         loaded = max(loaded, want)
@@ -543,7 +570,7 @@
             pltpu.VMEM((2, RING + 1, 8, HALF), F32),
             pltpu.VMEM((2, RING + 1, 8, HALF), F32),
             pltpu.VMEM((2, RING + 1, 8, HALF), F32),
-            dma((9,)),
+            dma((11,)),
             dma((len(GATHER),)), dma((len(GATHER),)),
             dma((len(CHAIN),)), dma((len(CHAIN),)),
             dma((2, RING)), dma((2, RING)),

time: 60.8 us -> 59.8 us (0.984)
  Pallas kernels: 60.1 us -> 58.9 us
    pallas_call x1, Pallas kernels: 58.8 us -> 57.7 us  [local(): pl.pallas_call(kernel, name='gated_backward', out_shape=(pltpu.VMEM((toke...]
where the time goes in v4:
time: 59.8 us; the launch traced here: 59.6 us
  Pallas kernels  58.9 us (98%)
  between operations  0.64 us (1%)
    pallas_call x1, Pallas kernels, local(): pl.pallas_call(kernel, name='gated_backward', out_shape=(pltpu.VMEM((toke...  57.7 us
    pallas_call x1, Pallas kernels, local(): pl.pallas_call(finish, name='finish', out_shape=(shape((tokens, width), B...  1.26 us

profile of v4, /device:TPU:6, one launch (start us, length us, event | category | flops | bytes accessed | tf_op | source)
XLA Modules:
  0.0 59.6 jit_solution(11251628412640020718)
XLA Ops:
  0.6 57.7 %gated_backward.1 = (bf16[768,512]{1,0:T(8,128)(2,1)S(1)}, bf16[768,512]{1,0:T(8,128)(2,1)S(1)}, f32[8,512]{1,0:T(8,128)S(1)}, f32[64,512]{1,0:T(8,128)S(1)}, f32[1,512]{1,0:T(1,128)S(1)}) custom-call(bf16[768,512]{1,0:T(8,128)(2,1)} %gate_hbm.1, bf16[768,512]{1,0:T(8,128)(2,1)} %linear_hbm.1, f32[3,512]{1,0:T(4,128)} %taps_g_hbm.1, f32[3,512]{1,0:T(4,128)} %taps_l_hbm.1, ...), custom_call_target="tpu_custom_call" | custom-call | tf_op jit(solution)/shard_map/gated_backward/pallas_call | solution.py:533
  58.3 1.3 %finish.1 = (bf16[768,512]{1,0:T(8,128)(2,1)}, bf16[768,512]{1,0:T(8,128)(2,1)}, f32[3,512]{1,0:T(4,128)}, f32[3,512]{1,0:T(4,128)}, f32[1,512]{1,0:T(1,128)}, /...) custom-call(bf16[768,512]{1,0:T(8,128)(2,1)S(1)} %get-tuple-element.21.gg, ...), custom_call_target="tpu_custom_call" | custom-call | tf_op jit(solution)/shard_map/finish/pallas_call | solution.py:592

commit v5 on v4

--- a/solution.py
+++ b/solution.py
@@ -100,7 +100,7 @@
         ]
 
     for i in range(4):
-        step(("w", i), 0.55, 2.5, [("w", i - 1)] if i else [("f", 1, 0), ("f", 1, 1)], start=2.5)
+        step(("w", i), 0.5, 2.5, [("w", i - 1)] if i else [("f", 1, 0), ("f", 1, 1)], start=2.5)
     follow = [1] * len(GATHER)
     for k in reversed(range(len(GATHER))):
         for n in GATHER[k][6]:
@@ -111,7 +111,7 @@
     for half in range(2):
         first, second = ("y", "z") if half == 0 else ("z", "y")
         for i in range(2):
-            step(("f", i, half), 0.5, 3 + i, [("f", 0, half)] * i, start=1.6 + 0.4 * i)
+            step(("f", i, half), 0.44, 3 + i, [("f", 0, half)] * i, start=1.6 + 0.4 * i)
         for k, (h, part, sign, at, hops) in enumerate(CHAIN):
             if h == half:
                 ready = ("w", part if half == 0 else Z_OFF.index(sign * (hops - at) % 4))
@@ -135,7 +135,7 @@
         for i in range(3):
             before = [("h", half, i - 1)] if i else every
             step(("h", half, i), 0.3, 5, before, () if i else every)
-            step(("b", half, i), 0.4, 5, [("h", half, i)] + [("b", half, i - 1)] * (i > 0), (),
+            step(("b", half, i), 0.35, 5, [("h", half, i)] + [("b", half, i - 1)] * (i > 0), (),
                  to_all("vy", half, "y", 8) if i == 2 else ())
         step(("ve", half), 0.1, 0.2, [("b", half, 2), ("ce", 1, 0)],
              [("vy", half, n) for n in FAR_FIRST], to_all("vz", half, "z", 8))
@@ -144,28 +144,28 @@
 
 
 ORDER = (
-    ("g", 32), ("g", 0), ("g", 4), ("g", 8), ("g", 40), ("g", 36), ("g", 1), ("g", 39),
-    ("f", 0, 0), ("f", 1, 0), ("f", 0, 1), ("f", 1, 1), ("w", 0), ("c", 4), ("c", 38), ("g", 43),
-    ("c", 52), ("g", 11), ("g", 33), ("c", 0), ("g", 14), ("g", 9), ("g", 42), ("g", 2),
-    ("c", 28), ("c", 42), ("w", 1), ("g", 3), ("g", 37), ("c", 32), ("c", 46), ("g", 18),
-    ("c", 7), ("c", 10), ("w", 2), ("g", 41), ("c", 49), ("c", 18), ("c", 14), ("c", 35),
-    ("w", 3), ("g", 55), ("c", 5), ("c", 24), ("c", 39), ("c", 21), ("g", 54), ("g", 34),
-    ("g", 46), ("g", 10), ("c", 53), ("g", 45), ("c", 29), ("c", 1), ("g", 38), ("c", 43),
-    ("g", 25), ("c", 33), ("c", 11), ("c", 8), ("c", 47), ("c", 19), ("c", 50), ("c", 15),
-    ("g", 44), ("c", 6), ("c", 36), ("c", 22), ("c", 40), ("c", 25), ("g", 57), ("g", 35),
-    ("g", 58), ("g", 28), ("g", 48), ("c", 2), ("c", 54), ("g", 22), ("c", 30), ("g", 19),
-    ("c", 34), ("c", 12), ("c", 44), ("c", 9), ("c", 48), ("c", 20), ("c", 51), ("c", 16),
-    ("g", 61), ("g", 15), ("c", 37), ("c", 23), ("c", 41), ("c", 26), ("g", 59), ("g", 5),
-    ("g", 52), ("g", 29), ("g", 51), ("c", 3), ("c", 55), ("g", 23), ("c", 31), ("g", 20),
-    ("g", 49), ("c", 13), ("c", 45), ("g", 26), ("g", 56), ("g", 60), ("c", 17), ("g", 62),
-    ("g", 16), ("g", 47), ("g", 12), ("ce", 1, 1), ("c", 27), ("g", 6), ("g", 30), ("g", 53),
-    ("ce", 0, 0), ("xs", 1, 1), ("ce", 1, 3), ("xs", 1, 3), ("ce", 1, 0), ("xs", 0, 0),
-    ("xs", 1, 0), ("g", 50), ("ce", 0, 1), ("xs", 0, 1), ("ce", 1, 2), ("xs", 1, 2), ("ce", 0, 2),
-    ("g", 27), ("xs", 0, 2), ("ce", 0, 3), ("xs", 0, 3), ("g", 13), ("g", 31), ("g", 7),
-    ("h", 1, 0), ("g", 17), ("h", 1, 1), ("g", 21), ("h", 1, 2), ("g", 24), ("b", 1, 0),
-    ("b", 1, 1), ("b", 1, 2), ("xe", 0), ("xe", 1), ("h", 0, 0), ("b", 0, 0), ("h", 0, 1),
-    ("h", 0, 2), ("b", 0, 1), ("b", 0, 2), ("ve", 1), ("ne", 0), ("ss", 0), ("ne", 1), ("ss", 1),
-    ("ve", 0), ("vo", 1), ("no", 0), ("so", 1), ("so", 0), ("no", 1), ("vo", 0),
+    ("g", 40), ("g", 36), ("g", 0), ("g", 1), ("g", 8), ("g", 32), ("g", 39), ("g", 4),
+    ("f", 0, 1), ("f", 0, 0), ("f", 1, 0), ("f", 1, 1), ("w", 0), ("c", 0), ("c", 4), ("c", 38),
+    ("c", 28), ("g", 37), ("g", 11), ("g", 55), ("g", 2), ("g", 33), ("c", 52), ("g", 54),
+    ("c", 42), ("g", 14), ("w", 1), ("g", 5), ("c", 7), ("g", 3), ("c", 46), ("g", 22), ("c", 32),
+    ("c", 10), ("w", 2), ("c", 14), ("c", 35), ("c", 18), ("c", 49), ("w", 3), ("c", 24),
+    ("c", 21), ("g", 43), ("c", 1), ("c", 5), ("g", 42), ("c", 39), ("c", 29), ("g", 56),
+    ("g", 45), ("c", 53), ("g", 34), ("g", 38), ("c", 43), ("g", 18), ("g", 28), ("c", 47),
+    ("c", 36), ("c", 8), ("c", 11), ("c", 33), ("c", 50), ("c", 15), ("c", 19), ("g", 46),
+    ("c", 22), ("g", 57), ("c", 25), ("c", 40), ("c", 30), ("c", 2), ("c", 6), ("g", 58),
+    ("g", 48), ("g", 35), ("g", 15), ("c", 54), ("c", 44), ("g", 25), ("g", 29), ("c", 48),
+    ("c", 37), ("c", 9), ("c", 12), ("c", 34), ("c", 51), ("c", 16), ("c", 20), ("g", 49),
+    ("c", 23), ("g", 60), ("c", 26), ("c", 41), ("c", 31), ("c", 3), ("g", 23), ("g", 61),
+    ("g", 51), ("g", 19), ("g", 16), ("c", 55), ("c", 45), ("g", 26), ("g", 30), ("g", 52),
+    ("g", 47), ("c", 13), ("g", 12), ("g", 44), ("c", 17), ("g", 41), ("g", 9), ("g", 50),
+    ("g", 59), ("c", 27), ("g", 6), ("ce", 1, 1), ("ce", 1, 0), ("ce", 0, 0), ("xs", 0, 0),
+    ("xs", 1, 0), ("xs", 1, 1), ("g", 62), ("ce", 1, 3), ("g", 20), ("xs", 1, 3), ("ce", 1, 2),
+    ("xs", 1, 2), ("g", 53), ("ce", 0, 1), ("xs", 0, 1), ("ce", 0, 2), ("xs", 0, 2), ("g", 13),
+    ("ce", 0, 3), ("xs", 0, 3), ("g", 27), ("g", 17), ("g", 7), ("g", 10), ("g", 31), ("g", 21),
+    ("h", 1, 0), ("h", 1, 1), ("g", 24), ("b", 1, 0), ("b", 1, 1), ("h", 1, 2), ("b", 1, 2),
+    ("xe", 1), ("xe", 0), ("h", 0, 0), ("h", 0, 1), ("h", 0, 2), ("b", 0, 0), ("b", 0, 1),
+    ("b", 0, 2), ("ve", 1), ("ne", 0), ("ss", 0), ("ne", 1), ("ss", 1), ("ve", 0), ("vo", 1),
+    ("no", 0), ("so", 1), ("so", 0), ("no", 1), ("vo", 0),
 )
 
 

time: 59.8 us -> 59.1 us (0.988)
  no operation moved by 1% of the time
where the time goes in v5:
time: 59.1 us; the launch traced here: 59 us
  Pallas kernels  58.4 us (99%)
  between operations  0.64 us (1%)
    pallas_call x1, Pallas kernels, local(): pl.pallas_call(kernel, name='gated_backward', out_shape=(pltpu.VMEM((toke...  57.1 us
    pallas_call x1, Pallas kernels, local(): pl.pallas_call(finish, name='finish', out_shape=(shape((tokens, width), B...  1.26 us

profile of v5, /device:TPU:6, one launch (start us, length us, event | category | flops | bytes accessed | tf_op | source)
XLA Modules:
  0.0 59.0 jit_solution(461223859061940378)
XLA Ops:
  0.6 57.1 %gated_backward.1 = (bf16[768,512]{1,0:T(8,128)(2,1)S(1)}, bf16[768,512]{1,0:T(8,128)(2,1)S(1)}, f32[8,512]{1,0:T(8,128)S(1)}, f32[64,512]{1,0:T(8,128)S(1)}, f32[1,512]{1,0:T(1,128)S(1)}) custom-call(bf16[768,512]{1,0:T(8,128)(2,1)} %gate_hbm.1, bf16[768,512]{1,0:T(8,128)(2,1)} %linear_hbm.1, f32[3,512]{1,0:T(4,128)} %taps_g_hbm.1, f32[3,512]{1,0:T(4,128)} %taps_l_hbm.1, ...), custom_call_target="tpu_custom_call" | custom-call | tf_op jit(solution)/shard_map/gated_backward/pallas_call | solution.py:533
  57.7 1.3 %finish.1 = (bf16[768,512]{1,0:T(8,128)(2,1)}, bf16[768,512]{1,0:T(8,128)(2,1)}, f32[3,512]{1,0:T(4,128)}, f32[3,512]{1,0:T(4,128)}, f32[1,512]{1,0:T(1,128)}, /...) custom-call(bf16[768,512]{1,0:T(8,128)(2,1)S(1)} %get-tuple-element.21.gg, ...), custom_call_target="tpu_custom_call" | custom-call | tf_op jit(solution)/shard_map/finish/pallas_call | solution.py:592

commit v6 on v5

--- a/solution.py
+++ b/solution.py
@@ -488,9 +488,13 @@
     loads[1].wait()
     pl.semaphore_wait(barrier, 4)
     loaded = 2
-    seen = []
+    seen, sent = [], []
     plan = steps()
     for name in ORDER:
+        if name[0] in ("no", "vo", "so"):
+            for done in [n for n in seen if n not in sent]:
+                message(done).wait_send()
+                sent.append(done)
         want = {"f": 8 + 2 * name[1], "w": 11}.get(name[0], 0)
         for load in loads[loaded:want]:
             load.wait()
@@ -500,7 +504,7 @@
                 message(needed).wait_recv()
                 seen.append(needed)
         run[name[0]](*name[1:])
-    for name in seen:
+    for name in [n for n in seen if n not in sent]:
         message(name).wait_send()
 
 

time: 59.1 us -> 58.8 us (level)
  no operation moved by 1% of the time
where the time goes in v6:
time: 58.8 us; the launch traced here: 58.7 us
  Pallas kernels  58.1 us (99%)
  between operations  0.64 us (1%)
    pallas_call x1, Pallas kernels, local(): pl.pallas_call(kernel, name='gated_backward', out_shape=(pltpu.VMEM((toke...  56.8 us
    pallas_call x1, Pallas kernels, local(): pl.pallas_call(finish, name='finish', out_shape=(shape((tokens, width), B...  1.26 us

profile of v6, /device:TPU:6, one launch (start us, length us, event | category | flops | bytes accessed | tf_op | source)
XLA Modules:
  0.0 58.7 jit_solution(8744687492315062953)
XLA Ops:
  0.6 56.8 %gated_backward.1 = (bf16[768,512]{1,0:T(8,128)(2,1)S(1)}, bf16[768,512]{1,0:T(8,128)(2,1)S(1)}, f32[8,512]{1,0:T(8,128)S(1)}, f32[64,512]{1,0:T(8,128)S(1)}, f32[1,512]{1,0:T(1,128)S(1)}) custom-call(bf16[768,512]{1,0:T(8,128)(2,1)} %gate_hbm.1, bf16[768,512]{1,0:T(8,128)(2,1)} %linear_hbm.1, f32[3,512]{1,0:T(4,128)} %taps_g_hbm.1, f32[3,512]{1,0:T(4,128)} %taps_l_hbm.1, ...), custom_call_target="tpu_custom_call" | custom-call | tf_op jit(solution)/shard_map/gated_backward/pallas_call | solution.py:537
  57.4 1.3 %finish.1 = (bf16[768,512]{1,0:T(8,128)(2,1)}, bf16[768,512]{1,0:T(8,128)(2,1)}, f32[3,512]{1,0:T(4,128)}, f32[3,512]{1,0:T(4,128)}, f32[1,512]{1,0:T(1,128)}, /...) custom-call(bf16[768,512]{1,0:T(8,128)(2,1)S(1)} %get-tuple-element.21.gg, ...), custom_call_target="tpu_custom_call" | custom-call | tf_op jit(solution)/shard_map/finish/pallas_call | solution.py:596
